TPU v7x, 512 devices: a whole 4x4x16 slice. The times are simulated.
512 devices in a mesh: sp: 16 (over z), fs: 4 (over y), tp: 8 (over x, core).
Axes of the slice: x: 4, y: 4, z: 16, core: 2. Of those that a mesh axis runs over, the one named last changes fastest.
Arguments:
- tokens: bfloat16 [16384, 2048], P(('fs', 'sp', 'tp')), parts along dimension 0, may hold values from -6 to 6
- norm_gain: float32 [2048], replicated, may hold values from 0.1 to 1.9
- recurrent_input: bfloat16 [2048, 1024], P(None, 'tp'), may hold values from -0.125 to 0.125
- recurrent_gate: bfloat16 [2048, 1024], P(None, 'tp'), may hold values from -0.125 to 0.125
- attention_gate: bfloat16 [2048, 1024], P(None, 'tp'), may hold values from -0.125 to 0.125
- query_proj: bfloat16 [2048, 1536], P(None, 'tp'), may hold values from -0.125 to 0.125
- latent_down: bfloat16 [2048, 512], P(None, 'tp'), may hold values from -0.125 to 0.125
- rope_key_down: bfloat16 [2048, 64], replicated, may hold values from -0.125 to 0.125
- conv_kernel: float32 [4, 1024], P(None, 'tp'), may hold values from -3 to 3
- recurrence_gate_blocks: bfloat16 [16, 64, 64], P('tp'), may hold values from -0.75 to 0.75
- input_gate_blocks: bfloat16 [16, 64, 64], P('tp'), may hold values from -0.75 to 0.75
- decay_rate: float32 [1024], P('tp'), as said below
- decay_shift: float32 [16384], P(('fs', 'sp')), parts along dimension 0, may hold values from -2 to 0, as said below
- initial_state: float32 [4096], P(('fs', 'tp')), parts along dimension 0, may hold values from -6 to 6
- latent_gain: float32 [512], replicated, may hold values from 0.1 to 1.9
- latent_up: bfloat16 [512, 2048], P(None, 'tp'), may hold values from -0.25 to 0.25
- query_gain: float32 [192], replicated, may hold values from 0.4 to 250, as said below
- recurrent_output: bfloat16 [1024, 2048], P('tp'), may hold values from -0.25 to 0.25
- attention_output: bfloat16 [1024, 2048], P('tp'), may hold values from -0.25 to 0.25
Outputs:
- mixed_output: bfloat16 [16384, 2048], P(('fs', 'sp', 'tp')), parts along dimension 0
There are 4 independent parts, one for each index of `fs`. A program takes and returns all parts, laid end to end along the dimension named above; an argument that names none is the same for every part. Nothing has to cross between parts.
Inputs may be any that keep to these rules, and one draw needn't show every extreme that they name: `decay_rate`: positive. `decay_shift`: negative. `query_gain`: positive.
All inputs are finite; a program needn't handle non-finite values.
Results may differ from a plain program's by a relative error of at most 0.03.
The roundings to bfloat16 on the way count: a program that leaves them out, or rounds other values in their place, can miss the bound.
Values may be sent and summed in bfloat16 or wider, within the bound.
A program may use at most 64 MiB of HBM per device.

v0:
```python
import math

import jax
import jax.numpy as jnp
from jax import lax
from jax.sharding import PartitionSpec as P

EPS = 1e-06
RECURRENT_SCALE = 8.0
THETA = 10000.0


def copy_for_each(shard, axis):
    copies = jnp.broadcast_to(shard, (lax.axis_size(axis), *shard.shape))
    return lax.all_to_all(copies, axis, split_axis=0, concat_axis=0, tiled=True)


def joined_along(blocks, dim):
    dims = list(blocks.shape[1:])
    dims[dim] *= blocks.shape[0]
    return jnp.moveaxis(blocks, 0, dim).reshape(dims)


def gather_directly(shard, axis, dim):
    blocks = copy_for_each(shard, axis)
    return joined_along(blocks, dim)


def from_behind(block, axis, distance):
    devices = range(lax.axis_size(axis))
    route = [(i - distance, i) for i in devices if i - distance in devices]
    return lax.ppermute(block, axis, route)


def gathered_once(shard, axis):
    leaves = jax.tree.leaves(shard)
    order = sorted(range(len(leaves)), key=lambda k: -leaves[k].size)
    width = (1, *leaves[order[0]].shape)[-1]
    lines = [
        jnp.pad(leaves[k].reshape(-1), (0, -leaves[k].size % width)).reshape(-1, width)
        for k in order
    ]
    both, at, found = (copy_for_each(jnp.concatenate(lines), axis), 0, {})
    for k, line in zip(order, lines):
        share = both[:, at : at + len(line)].reshape(len(both), -1)
        found[k] = share[:, : leaves[k].size].reshape(-1, *leaves[k].shape)
        at += len(line)
    numbers = iter(range(len(leaves)))
    return jax.tree.map(lambda _: found[next(numbers)], shard)


def joined_by_halves(pieces, combine):
    while len(jax.tree.leaves(pieces)[0]) > 1:
        pieces = jax.vmap(combine)(
            *(jax.tree.map(lambda part: part[side::2], pieces) for side in (0, 1))
        )
    return jax.tree.map(lambda part: part[0], pieces)


def prefix(shard, axis, combine, identity):
    count, position = (lax.axis_size(axis), lax.axis_index(axis))
    passed = jnp.arange(count) < position

    def kept(part, zero, own):
        part = jnp.where(
            passed.reshape(-1, *(1 for _ in own.shape)), part, jnp.asarray(zero, own.dtype)
        )
        return part

    pieces = gathered_once(shard, axis)
    return joined_by_halves(jax.tree.map(kept, pieces, identity, shard), combine)


def sent_together(arrays, axis, dim, along):
    ends, at = ([], 0)
    for a in arrays[:-1]:
        at += a.shape[along]
        ends.append(at)
    both = jnp.concatenate(arrays, axis=along)
    return tuple(jnp.split(lax.all_gather(both, axis, axis=dim, tiled=True), ends, axis=along))


def in_blocks(shard, dim, count):
    before, after = (shard.shape[:dim], shard.shape[dim + 1 :])
    return jnp.moveaxis(shard.reshape(*before, count, -1, *after), dim, 0)


def summed_on_arrival(shard, axis, dim):
    count = lax.axis_size(axis)
    blocks = lax.all_to_all(in_blocks(shard, dim, count), axis, 0, 0, tiled=True)
    return jnp.sum(blocks.astype(jnp.float32), axis=0)


def rotate_half(values, token_positions):
    half_width = values.shape[-1] // 2
    inv_freq = 1.0 / THETA ** (
        jnp.arange(0, 2 * half_width, 2, dtype=jnp.float32) / (2 * half_width)
    )
    angles = token_positions.astype(jnp.float32)[:, None] * inv_freq[None, :]
    cosine = jnp.cos(angles)
    sine_part = jnp.sin(angles)
    if values.ndim == 3:
        cosine = cosine[:, None, :]
        sine_part = sine_part[:, None, :]
    first_half = values[..., :half_width]
    second_half = values[..., half_width:]
    return jnp.concatenate(
        [
            first_half * cosine - second_half * sine_part,
            first_half * sine_part + second_half * cosine,
        ],
        axis=-1,
    )


def rms_scaled(values, gain_vec):
    return values * lax.rsqrt(jnp.mean(values * values, axis=-1, keepdims=True) + EPS) * gain_vec


def linear_step(earlier, later_part):
    return (earlier[0] * later_part[0], later_part[0] * earlier[1] + later_part[1])


def body(
    tokens,
    norm_gain,
    recurrent_input,
    recurrent_gate,
    attention_gate,
    query_proj,
    latent_down,
    rope_key_down,
    conv_kernel,
    recurrence_gate_blocks,
    input_gate_blocks,
    decay_rate,
    decay_shift,
    initial_state,
    latent_gain,
    latent_up,
    query_gain,
    recurrent_output,
    attention_output,
):
    sp_count = lax.axis_size("sp")
    sp_place = lax.axis_index("sp")
    channel_width = recurrent_input.shape[1]
    value_width = attention_gate.shape[1]
    query_width = query_proj.shape[1]
    latent_width = latent_down.shape[1]
    rope_width = rope_key_down.shape[1]
    head_dim = query_gain.shape[0]
    nope_width = head_dim - rope_width
    local_heads = query_width // head_dim
    head_value = value_width // local_heads
    joined_weight = jnp.concatenate(
        [recurrent_input, recurrent_gate, attention_gate, query_proj, latent_down, rope_key_down],
        axis=1,
    )
    normed = rms_scaled(gather_directly(tokens, "tp", 0).astype(jnp.float32), norm_gain).astype(
        jnp.bfloat16
    )
    projected = jnp.dot(normed, joined_weight, preferred_element_type=jnp.float32).astype(
        jnp.bfloat16
    )
    local_tokens = projected.shape[0]
    split_points = []
    running_total = 0
    for width_part in [channel_width, channel_width, value_width, query_width, latent_width]:
        running_total += width_part
        split_points.append(running_total)
    recur_signal, recur_gate_pre, attention_pre, query_raw, latent_local, rope_raw = jnp.split(
        projected, split_points, axis=1
    )
    token_positions = sp_place * local_tokens + jnp.arange(local_tokens, dtype=jnp.int32)
    taps = conv_kernel.shape[0]
    conv_rim = from_behind(recur_signal[local_tokens - taps + 1 :], "sp", 1)
    extended = jnp.concatenate([conv_rim, recur_signal], axis=0).astype(jnp.float32)
    conv_sum = conv_kernel[0] * extended[0:local_tokens]
    for tap_index in range(1, taps):
        conv_sum = (
            conv_sum + conv_kernel[tap_index] * extended[tap_index : tap_index + local_tokens]
        )
    conv_out = conv_sum.astype(jnp.bfloat16)
    block_size = recurrence_gate_blocks.shape[1]
    grouped = conv_out.reshape(local_tokens, channel_width // block_size, block_size)
    recur_rate = jax.nn.sigmoid(
        jnp.einsum(
            "tbi,bij->tbj", grouped, recurrence_gate_blocks, preferred_element_type=jnp.float32
        ).reshape(local_tokens, channel_width)
    )
    input_rate = jax.nn.sigmoid(
        jnp.einsum(
            "tbi,bij->tbj", grouped, input_gate_blocks, preferred_element_type=jnp.float32
        ).reshape(local_tokens, channel_width)
    )
    log_decay = -RECURRENT_SCALE * recur_rate * decay_rate + decay_shift[:, None]
    decay = jnp.exp(log_decay)
    driven = jnp.sqrt(-jnp.expm1(2.0 * log_decay)) * input_rate * conv_out.astype(jnp.float32)
    decay_prod, zero_state = lax.associative_scan(linear_step, (decay, driven), axis=0)
    carry_decay, carry_state = prefix(
        (decay_prod[-1], zero_state[-1]),
        "sp",
        linear_step,
        (jnp.ones_like(initial_state), jnp.zeros_like(initial_state)),
    )
    incoming = carry_decay * initial_state + carry_state
    states = zero_state + decay_prod * incoming
    recur_out = (states * jax.nn.silu(recur_gate_pre.astype(jnp.float32))).astype(jnp.bfloat16)
    query_rows = rms_scaled(
        query_raw.astype(jnp.float32).reshape(local_tokens, local_heads, head_dim), query_gain
    )
    query_rows = jnp.concatenate(
        [query_rows[..., :nope_width], rotate_half(query_rows[..., nope_width:], token_positions)],
        axis=-1,
    ).astype(jnp.bfloat16)
    query_nope = query_rows[..., :nope_width]
    query_rope = query_rows[..., nope_width:]
    latent_rows = gather_directly(latent_local, "tp", 1)
    normed_latent = rms_scaled(latent_rows.astype(jnp.float32), latent_gain).astype(jnp.bfloat16)
    own_expanded = jnp.dot(normed_latent, latent_up, preferred_element_type=jnp.float32).astype(
        jnp.bfloat16
    )
    own_rope = rotate_half(rope_raw.astype(jnp.float32), token_positions).astype(jnp.bfloat16)
    expanded, key_rope = sent_together((own_expanded, own_rope), "sp", 0, 1)
    key_count = expanded.shape[0]
    key_positions = jnp.arange(key_count, dtype=jnp.int32)
    head_keys = expanded.reshape(key_count, local_heads, nope_width + head_value)
    key_nope = head_keys[..., :nope_width]
    key_values = head_keys[..., nope_width:]
    key_group = math.gcd(sp_count, 4)
    block_keys = local_tokens * key_group
    block_total = key_count // block_keys
    score_scale = head_dim ** (-0.5)

    def online_step(block_index, carried):
        running_max, total_weight, weighted = carried
        begin_key = block_index * block_keys
        nope_block = lax.dynamic_slice_in_dim(key_nope, begin_key, block_keys, 0)
        rope_block = lax.dynamic_slice_in_dim(key_rope, begin_key, block_keys, 0)
        pos_block = lax.dynamic_slice_in_dim(key_positions, begin_key, block_keys, 0)
        value_block = lax.dynamic_slice_in_dim(key_values, begin_key, block_keys, 0)
        scores = jnp.einsum(
            "thd,khd->htk", query_nope, nope_block, preferred_element_type=jnp.float32
        )
        scores = scores + jnp.einsum(
            "thr,kr->htk", query_rope, rope_block, preferred_element_type=jnp.float32
        )
        scores = scores * score_scale
        allowed = pos_block[None, :] <= token_positions[:, None]
        scores = jnp.where(allowed[None], scores, -jnp.inf)
        new_max = jnp.maximum(running_max, jnp.max(scores, axis=-1))
        rescale = jnp.exp(running_max - new_max)
        weights = jnp.exp(scores - new_max[..., None])
        block_weighted = jnp.einsum(
            "htk,khd->thd",
            weights.astype(jnp.bfloat16),
            value_block,
            preferred_element_type=jnp.float32,
        )
        weighted = weighted * jnp.transpose(rescale)[:, :, None] + block_weighted
        total_weight = total_weight * rescale + jnp.sum(weights, axis=-1)
        return (new_max, total_weight, weighted)

    start_sums = (
        jnp.full((local_heads, local_tokens), -jnp.inf, jnp.float32),
        jnp.zeros((local_heads, local_tokens), jnp.float32),
        jnp.zeros((local_tokens, local_heads, head_value), jnp.float32),
    )
    row_max, total_weight, weighted = lax.fori_loop(0, block_total, online_step, start_sums)
    attended = weighted / jnp.transpose(total_weight)[:, :, None]
    attention_out = (
        attended.reshape(local_tokens, value_width) * jax.nn.silu(attention_pre.astype(jnp.float32))
    ).astype(jnp.bfloat16)
    summed = summed_on_arrival(
        (
            jnp.dot(recur_out, recurrent_output, preferred_element_type=jnp.float32)
            + jnp.dot(attention_out, attention_output, preferred_element_type=jnp.float32)
        ).astype(jnp.bfloat16),
        "tp",
        0,
    )
    return summed.astype(jnp.bfloat16)


def solution(mesh):
    return jax.shard_map(
        body,
        mesh=mesh,
        in_specs=(
            P(("fs", "sp", "tp"), None),
            P(),
            P(None, "tp"),
            P(None, "tp"),
            P(None, "tp"),
            P(None, "tp"),
            P(None, "tp"),
            P(),
            P(None, "tp"),
            P("tp", None, None),
            P("tp", None, None),
            P("tp"),
            P(("fs", "sp")),
            P(("fs", "tp")),
            P(),
            P(None, "tp"),
            P(),
            P("tp", None),
            P("tp", None),
        ),
        out_specs=P(("fs", "sp", "tp"), None),
        check_vma=False,
    )
```

profile of v0, /device:TPU:1, one launch (start us, length us, event | category | flops | bytes accessed | tf_op | source)
XLA Modules:
  0.0 198.2 jit_solution(5296528355386771109)
XLA Ops:
  6.5 2.1 %broadcast_in_dim.73 = bf16[8,32,2048]{2,1,0:T(8,128)(2,1)} broadcast(bf16[32,2048]{1,0:T(8,128)(2,1)} %param.21), dimensions={1,2} | broadcast | bytes 1179648 | tf_op jit(solution)/shard_map/broadcast_in_dim | solution.py:14
  8.6 10.3 %all-to-all-start = ((bf16[8,32,2048]{2,1,0:T(8,128)(2,1)}), bf16[8,32,2048]{2,1,0:T(8,128)(2,1)S(1)}, u32[]{:S(2)}, u32[]{:S(2)}) async-start(bf16[8,32,2048]{2,1,0:T(8,128)(2,1)} %broadcast_in_dim.73), calls=%async_computation | async-start | bytes 2097152 | tf_op jit(solution)/shard_map/all_to_all | solution.py:15
  29.6 4.3 %all-to-all-done = bf16[8,32,2048]{2,1,0:T(8,128)(2,1)S(1)} async-done(((bf16[8,32,2048]{2,1,0:T(8,128)(2,1)}), bf16[8,32,2048]{2,1,0:T(8,128)(2,1)S(1)}, u32[]{:S(2)}, u32[]{:S(2)}) %all-to-all-start) | async-done | bytes 1048608 | tf_op jit(solution)/shard_map/all_to_all | solution.py:15
  34.7 2.8 %convolution_convert_fusion = bf16[256,704]{0,1:T(8,128)(2,1)S(1)} fusion(bf16[256,2048]{1,0:T(8,128)(2,1)S(1)} %fusion.26, bf16[2048,704]{0,1:T(8,128)(2,1)} %constant_dynamic-update-slice_fusion), kind=kOutput, calls=%fused_computation.38 | convolution fusion | flops 738377728 | bytes 4292608 | tf_op jit(solution)/shard_map/dot_general | solution.py:163
  40.4 4.3 %all-to-all-start.2 = ((bf16[8,256,64]{1,2,0:T(8,128)(2,1)}), bf16[8,256,64]{1,2,0:T(8,128)(2,1)S(1)}, u32[]{:S(2)}, u32[]{:S(2)}) async-start(bf16[8,256,64]{1,2,0:T(8,128)(2,1)} %broadcast_in_dim.81), calls=%async_computation.2 | async-start | bytes 524288 | tf_op jit(solution)/shard_map/all_to_all | solution.py:15
  46.0 2.2 %slice.363 = f32[128,128]{0,1:T(8,128)S(1)} slice(f32[256,128]{0,1:T(8,128)S(1)} %get-tuple-element.307), slice={[1:256:2], [0:128:1]} | slice | bytes 131072 | tf_op jit(solution)/shard_map/slice | solution.py:200
  48.2 2.2 %slice.362 = f32[128,128]{0,1:T(8,128)S(1)} slice(f32[256,128]{0,1:T(8,128)S(1)} %get-tuple-element.307), slice={[0:255:2], [0:128:1]} | slice | bytes 131072 | tf_op jit(solution)/shard_map/slice | solution.py:200
  50.5 2.2 %slice.365 = f32[128,128]{0,1:T(8,128)S(1)} slice(f32[256,128]{0,1:T(8,128)S(1)} %get-tuple-element.308), slice={[0:255:2], [0:128:1]} | slice | bytes 131072 | tf_op jit(solution)/shard_map/slice | solution.py:200
  52.7 2.2 %slice.361 = f32[128,128]{0,1:T(8,128)S(1)} slice(f32[256,128]{0,1:T(8,128)S(1)} %get-tuple-element.308), slice={[1:256:2], [0:128:1]} | slice | bytes 131072 | tf_op jit(solution)/shard_map/slice | solution.py:200
  68.1 2.2 %slice.417 = f32[127,128]{0,1:T(8,128)S(1)} slice(f32[256,128]{0,1:T(8,128)S(1)} %get-tuple-element.307), slice={[2:256:2], [0:128:1]} | slice | bytes 130048 | tf_op jit(solution)/shard_map/slice | solution.py:200
  70.3 2.2 %slice.360 = f32[127,128]{0,1:T(8,128)S(1)} slice(f32[256,128]{0,1:T(8,128)S(1)} %get-tuple-element.308), slice={[2:256:2], [0:128:1]} | slice | bytes 130048 | tf_op jit(solution)/shard_map/slice | solution.py:200
  89.2 2.2 %pad.128 = f32[256,128]{0,1:T(8,128)S(1)} pad(f32[128,128]{0,1:T(8,128)S(1)} %pad_maximum_fusion.11, f32[]{:T(128)} %constant.80.clone.1), padding=0_1_1x0_0_0 | pad | bytes 196612 | tf_op jit(solution)/shard_map/pad | solution.py:200
  91.5 2.2 %pad.112 = f32[256,128]{0,1:T(8,128)S(1)} pad(f32[128,128]{0,1:T(8,128)S(1)} %pad_maximum_fusion.4, f32[]{:T(128)} %constant.80.clone.1), padding=0_1_1x0_0_0 | pad | bytes 196612 | tf_op jit(solution)/shard_map/pad | solution.py:200
  93.7 2.4 %pad.113 = f32[256,128]{0,1:T(8,128)S(1)} pad(f32[128,128]{0,1:T(8,128)S(1)} %add.335, f32[]{:T(128)} %constant.80.clone.1), padding=1_0_1x0_0_0 | pad | bytes 196612 | tf_op jit(solution)/shard_map/pad | solution.py:200
  96.0 2.2 %pad.129 = f32[256,128]{0,1:T(8,128)S(1)} pad(f32[128,128]{0,1:T(8,128)S(1)} %add.344, f32[]{:T(128)} %constant.80.clone.1), padding=1_0_1x0_0_0 | pad | bytes 196612 | tf_op jit(solution)/shard_map/pad | solution.py:200
  99.2 12.0 %all-to-all-start.1 = ((f32[16,2,128]{2,1,0:T(2,128)}), f32[16,2,128]{2,1,0:T(2,128)S(1)}, u32[]{:S(2)}, u32[]{:S(2)}) async-start(f32[16,2,128]{2,1,0:T(2,128)} %broadcast_in_dim.75), calls=%async_computation.1 | async-start | bytes 32768 | tf_op jit(solution)/shard_map/all_to_all | solution.py:15
  111.3 11.6 %all-to-all-done.1 = f32[16,2,128]{2,1,0:T(2,128)S(1)} async-done(((f32[16,2,128]{2,1,0:T(2,128)}), f32[16,2,128]{2,1,0:T(2,128)S(1)}, u32[]{:S(2)}, u32[]{:S(2)}) %all-to-all-start.1) | async-done | bytes 16416 | tf_op jit(solution)/shard_map/all_to_all | solution.py:15
  123.3 1.4 fusion.56
  124.6 16.6 %all-gather.2.cloned.1.call-done = bf16[4096,320]{0,1:T(8,128)(2,1)} async-done(((bf16[256,320]{0,1:T(8,128)(2,1)}), bf16[4096,320]{0,1:T(8,128)(2,1)}) %all-gather.2.cloned.1.call-update) | async-done | bytes 2621456 | tf_op jit(solution)/shard_map/all_gather | solution.py:80
  141.3 1.7 slice_bitcast_fusion
  143.0 1.5 fusion.87
  144.5 13.1 %while.18 = (s32[]{:T(128)}, f32[1,256]{1,0:T(1,128)S(1)}, f32[1,256]{1,0:T(1,128)S(1)}, f32[256,1,128]{0,2,1:T(8,128)S(1)}, s32[4096]{0:T(1024)S(1)}, /*index=5...) while((s32[]{:T(128)}, f32[1,256]{1,0:T(1,128)S(1)}, ...), condition=%wide.region_6.7_spmd.clone, body=%wide.region_3.6_spmd.clone.sunk | while | flops 170231296 | bytes 6289635 | solution.py:270
  157.6 1.6 fusion.24
  159.2 31.2 %all_to_all.20 = bf16[8,32,2048]{2,1,0:T(8,128)(2,1)S(1)} all-to-all(bf16[8,32,2048]{2,1,0:T(8,128)(2,1)S(1)} %bitcast.145), channel_id=1, replica_groups=mesh['sp'=16,'fs'=4,'tp'=8] {'tp'}, dimensions={0} | all-to-all | bytes 2097152 | tf_op jit(solution)/shard_map/all_to_all | solution.py:90
  (269 shorter events, 59.5 us)
Async XLA Ops:
  6.5 116.7 %copy-start = (bf16[128,2048]{1,0:T(8,128)(2,1)S(1)}, bf16[128,2048]{1,0:T(8,128)(2,1)}, u32[]{:S(2)}) copy-start(bf16[128,2048]{1,0:T(8,128)(2,1)} %param.38) | copy-start | bytes 1572868
  6.5 14.1 %copy-start.13 = (f32[4,128]{1,0:T(4,128)S(1)}, f32[4,128]{1,0:T(4,128)}, u32[]{:S(2)}) copy-start(f32[4,128]{1,0:T(4,128)} %param.29) | copy-start | bytes 6148
  6.5 14.6 %copy-start.3 = (bf16[2048,128]{1,0:T(8,128)(2,1)S(1)}, bf16[2048,128]{1,0:T(8,128)(2,1)}, u32[]{:S(2)}) copy-start(bf16[2048,128]{1,0:T(8,128)(2,1)} %param.23) | copy-start | bytes 1572868
  8.6 25.3 %all-to-all-start = ((bf16[8,32,2048]{2,1,0:T(8,128)(2,1)}), bf16[8,32,2048]{2,1,0:T(8,128)(2,1)S(1)}, u32[]{:S(2)}, u32[]{:S(2)}) async-start(bf16[8,32,2048]{2,1,0:T(8,128)(2,1)} %broadcast_in_dim.73), calls=%async_computation | async-start | bytes 2097152 | tf_op jit(solution)/shard_map/all_to_all | solution.py:15
  22.6 5.5 %copy-start.4 = (bf16[2048,64]{0,1:T(8,128)(2,1)S(1)}, bf16[2048,64]{0,1:T(8,128)(2,1)}, u32[]{:S(2)}) copy-start(bf16[2048,64]{0,1:T(8,128)(2,1)} %param.27) | copy-start | bytes 786436
  23.9 3.2 %copy-start.1 = (bf16[2048,192]{0,1:T(8,128)(2,1)S(1)}, bf16[2048,192]{0,1:T(8,128)(2,1)}, u32[]{:S(2)}) copy-start(bf16[2048,192]{0,1:T(8,128)(2,1)} %param.26) | copy-start | bytes 2359300
  23.9 4.9 %copy-start.5 = (bf16[2048,64]{0,1:T(8,128)(2,1)S(1)}, bf16[2048,64]{0,1:T(8,128)(2,1)}, u32[]{:S(2)}) copy-start(bf16[2048,64]{0,1:T(8,128)(2,1)} %param.28) | copy-start | bytes 786436
  24.8 9.5 %copy-start.7 = (f32[2048]{0:T(1024)S(1)}, f32[2048]{0:T(1024)}, u32[]{:S(2)}) copy-start(f32[2048]{0:T(1024)} %param.22) | copy-start | bytes 24580
  34.6 4.4 %copy-start.14 = (f32[192]{0:T(256)S(1)}, f32[192]{0:T(256)}, u32[]{:S(2)}) copy-start(f32[192]{0:T(256)} %param.37) | copy-start | bytes 2308
  34.6 4.5 %copy-start.10 = (f32[256]{0:T(256)S(1)}, f32[256]{0:T(256)}, u32[]{:S(2)}) copy-start(f32[256]{0:T(256)} %add_convert_fusion) | copy-start | bytes 3076
  34.6 4.5 %copy-start.12 = (f32[32]{0:T(128)S(1)}, f32[32]{0:T(128)}, u32[]{:S(2)}) copy-start(f32[32]{0:T(128)} %negate_power_fusion) | copy-start | bytes 388
  34.6 10.3 %copy-start.8 = (f32[128]{0:T(128)S(1)}, f32[128]{0:T(128)}, u32[]{:S(2)}) copy-start(f32[128]{0:T(128)} %get-tuple-element.354) | copy-start | bytes 1540
  34.6 10.3 %copy-start.9 = (f32[128]{0:T(128)S(1)}, f32[128]{0:T(128)}, u32[]{:S(2)}) copy-start(f32[128]{0:T(128)} %get-tuple-element.355) | copy-start | bytes 1540
  34.7 10.6 %copy-start.18 = (bf16[2,64,64]{2,1,0:T(8,128)(2,1)S(1)}, bf16[2,64,64]{2,1,0:T(8,128)(2,1)}, u32[]{:S(2)}) copy-start(bf16[2,64,64]{2,1,0:T(8,128)(2,1)} %param.31) | copy-start | bytes 49156
  37.5 8.0 %copy-start.19 = (bf16[2,64,64]{2,1,0:T(8,128)(2,1)S(1)}, bf16[2,64,64]{2,1,0:T(8,128)(2,1)}, u32[]{:S(2)}) copy-start(bf16[2,64,64]{2,1,0:T(8,128)(2,1)} %param.30) | copy-start | bytes 49156
  37.5 8.2 %copy-start.15 = (f32[256]{0:T(256)S(1)}, f32[256]{0:T(256)}, u32[]{:S(2)}) copy-start(f32[256]{0:T(256)} %param.33) | copy-start | bytes 3076
  37.7 7.2 %collective-permute-start = (bf16[3,128]{0,1:T(8,128)(2,1)S(1)}, bf16[3,128]{0,1:T(8,128)(2,1)S(1)}, u32[]{:S(2)}, u32[]{:S(2)}) collective-permute-start(bf16[3,128]{0,1:T(8,128)(2,1)S(1)} %slice.460), channel_id=1, source_target_pairs={{0,32},{32,64},{64,96},{96,128},{128,160},{160,192},{192,224},{224... | collective-permute-start | bytes 2312 | tf_op jit(solution)/shard_map/ppermute | solution.py:32
  40.4 26.4 %all-to-all-start.2 = ((bf16[8,256,64]{1,2,0:T(8,128)(2,1)}), bf16[8,256,64]{1,2,0:T(8,128)(2,1)S(1)}, u32[]{:S(2)}, u32[]{:S(2)}) async-start(bf16[8,256,64]{1,2,0:T(8,128)(2,1)} %broadcast_in_dim.81), calls=%async_computation.2 | async-start | bytes 524288 | tf_op jit(solution)/shard_map/all_to_all | solution.py:15
  44.7 96.6 %all-gather.2.cloned.1.call-start = ((), (), s32[]{:S(2)}) async-start(), calls=%async_computation.4 | async-start | bytes 2785280 | tf_op jit(solution)/shard_map/all_gather | solution.py:80
  63.8 3.1 %copy-start.11 = (f32[512]{0:T(512)S(1)}, f32[512]{0:T(512)}, u32[]{:S(2)}) copy-start(f32[512]{0:T(512)} %param.35) | copy-start | bytes 6148
  64.4 2.7 %copy-start.6 = (bf16[512,256]{1,0:T(8,128)(2,1)S(1)}, bf16[512,256]{1,0:T(8,128)(2,1)}, u32[]{:S(2)}) copy-start(bf16[512,256]{1,0:T(8,128)(2,1)} %param.36) | copy-start | bytes 786436
  82.8 40.1 %copy-start.16 = (pred[16]{0:T(512)(128)(4,1)S(1)}, pred[16]{0:T(512)(128)(4,1)}, u32[]{:S(2)}) copy-start(pred[16]{0:T(512)(128)(4,1)} %iota_compare_fusion) | copy-start | bytes 52
  82.8 40.5 %copy-start.17 = (f32[128]{0:T(128)S(1)}, f32[128]{0:T(128)}, u32[]{:S(2)}) copy-start(f32[128]{0:T(128)} %param.34) | copy-start | bytes 1540
  99.2 23.6 %all-to-all-start.1 = ((f32[16,2,128]{2,1,0:T(2,128)}), f32[16,2,128]{2,1,0:T(2,128)S(1)}, u32[]{:S(2)}, u32[]{:S(2)}) async-start(f32[16,2,128]{2,1,0:T(2,128)} %broadcast_in_dim.75), calls=%async_computation.1 | async-start | bytes 32768 | tf_op jit(solution)/shard_map/all_to_all | solution.py:15
  (2 other events, 3.6 us)
Sparse Core Ops, SparseCore 0:
  68.2 73.0 all-gather.1
where the time goes:
time: 202 us; the launch traced here: 198 us
  local copies, waits for them, and re-layouts  64.1 us (32%)
  waiting for transfers between devices  32.6 us (16%)
  blocking collectives  31.2 us (15%)
  starting transfers between devices  28 us (14%)
  matrix products  18.3 us (9%)
  between operations  14.8 us (7%)
  other arithmetic  8.94 us (4%)
    all_to_all x1, blocking collectives, summed_on_arrival(): lax.all_to_all(in_blocks(shard, dim, count), axis, 0, 0, tiled=True)  31.2 us
    slice x42, local copies, waits for them, and re-layouts, body(): lax.associative_scan(linear_step, (decay, driven), axis=0)  28.2 us
    all_to_all x3, starting transfers between devices, copy_for_each(): return lax.all_to_all(copies, axis, split_axis=0, concat_axis=0, tiled=True)  26.6 us
    pad x28, local copies, waits for them, and re-layouts, body(): lax.associative_scan(linear_step, (decay, driven), axis=0)  19.2 us
    all_gather x1, waiting for transfers between devices, sent_together(): lax.all_gather(both, axis, axis=dim, tiled=True)  16.6 us
    all_to_all x3, waiting for transfers between devices, copy_for_each(): return lax.all_to_all(copies, axis, split_axis=0, concat_axis=0, tiled=True)  16 us
    unnamed x55, local copies, waits for them, and re-layouts  7.66 us
    dot_general x4, matrix products, online_step(): jnp.einsum('htk,khd->thd', weights.astype(jnp.bfloat16), value_block, pre...  5.13 us
  transfers between devices with their start and end apart: 5, of which 3 were waited for; matrix products, arithmetic and copies ran while one was open for 33% of the time, Pallas kernels for 0%

commit v1 on v0

v1 whole, which is shorter than its diff:
```python
import functools

import jax
import jax.numpy as jnp
import numpy as np
from jax import lax
from jax.experimental import pallas as pl
from jax.experimental.pallas import tpu as pltpu
from jax.sharding import PartitionSpec as P

MESH = pl.DeviceIdType.MESH
EPS = 1e-06
THETA = 10000.0
F32, BF16 = jnp.float32, jnp.bfloat16
NZ, NX, TOK, D = 16, 4, 256, 2048
PIECES, ROWS = 4, 160
NT = (((1,), (1,)), ((), ()))


def dot(a, b):
    return jnp.dot(a, b, preferred_element_type=F32)


def silu(v):
    return v * jax.nn.sigmoid(v)


def minus_expm1(y):
    series = 1.0 + y * (1.0 / 8.0)
    for n in (7, 6, 5, 4, 3, 2):
        series = 1.0 + y * (1.0 / n) * series
    return jnp.where(y > -0.35, -y * series, 1.0 - jnp.exp(y))


def rotary_tables():
    inv = 1.0 / THETA ** (np.arange(0, 64, 2, dtype=np.float64) / 64)
    lanes = np.tile(inv, 4)

    def table(positions):
        angles = positions[:, None].astype(np.float64) * lanes[None]
        return np.concatenate([np.cos(angles), np.sin(angles)], 1).astype(np.float32)

    return table(np.arange(TOK)), table(TOK * np.arange(NZ))


def kernel(
    tok_h, ngain_h, rin_h, rgate_h, agate_h, wq_h, wlat_h, wrk_h, conv_h, rblk_h, iblk_h,
    drate_h, dshift_h, init_h, lgain_h, lup_h, qgain_h, rout_h, aout_h, base_h, far_h,
    out_ref,
    tok, ngain, wa, wb, wq, wlat, wrk, conv, rblk, iblk, drate, dshift, init, lgain, lup,
    qgain, wo, base, far,
    xbuf, latbuf, halo_tx, halo_rx, kvbuf, cbuf, qn_s, qlo_s, qhi_s, acc_s, ml_s,
    a_s, b_s, gate_s, agate_s, xrow, xcat, d2d_tx, d2d_rx, psum, rtx, rrx,
    in_sem, g_ssem, g_rsem, d_ssem, d_rsem, l_ssem, l_rsem, ld_ssem, ld_rsem, h_sem,
    kv_ssem, kv_rsem, c_ssem, c_rsem, o_ssem, o_rsem, r_ssem, r_rsem,
):
    z = lax.axis_index("sp")
    t = lax.axis_index("tp")
    x, c = lax.div(t, 2), lax.rem(t, 2)

    def chip(offset):
        return lax.rem(x + (offset + NX), NX)

    def tp_of(xx, cc):
        return 2 * xx + cc

    def zat(offset):
        return lax.rem(z + (offset + 2 * NZ), NZ)

    partner = {"tp": tp_of(x, 1 - c)}
    xup, xdn, xfar = ({"tp": tp_of(chip(o), c)} for o in (1, -1, 2))
    zup, zdn = {"sp": zat(1)}, {"sp": zat(-1)}
    started = []

    def remote(src, dst, ssem, rsem, to):
        return pltpu.make_async_remote_copy(
            src_ref=src, dst_ref=dst, send_sem=ssem, recv_sem=rsem, device_id=to,
            device_id_type=MESH,
        )

    def send(src, dst, ssem, rsem, to):
        copy = remote(src, dst, ssem, rsem, to)
        copy.start()
        started.append(copy)

    def arrived(dst, rsem, to=None):
        remote(dst, dst, rsem, rsem, partner).wait_recv()

    barrier = pltpu.get_barrier_semaphore()
    for peer in (partner, xup, xdn, xfar, zup, zdn):
        pl.semaphore_signal(barrier, inc=1, device_id=peer, device_id_type=MESH)

    loads = [
        (tok_h, tok), (ngain_h, ngain), (wq_h, wq), (wlat_h, wlat), (wrk_h, wrk),
        (rin_h, wa.at[:, 0:128]), (rgate_h, wa.at[:, 128:256]), (agate_h, wa.at[:, 256:384]),
        (conv_h, conv), (rblk_h, rblk), (iblk_h, iblk), (drate_h, drate), (dshift_h, dshift),
        (init_h, init), (lgain_h, lgain), (lup_h, lup), (qgain_h, qgain),
        (rout_h, wo.at[0:128]), (aout_h, wo.at[128:256]), (base_h, base), (far_h, far),
    ]
    copies = [pltpu.make_async_copy(s, d, in_sem.at[k]) for k, (s, d) in enumerate(loads)]
    for copy in copies:
        copy.start()

    copies[0].wait()
    copies[1].wait()
    own = tok[...].astype(F32)
    own = own * lax.rsqrt(jnp.mean(own * own, axis=1, keepdims=True) + EPS) * ngain[...]
    own_at = pl.multiple_of(32 * t, 32)
    xbuf[pl.ds(own_at, 32), :] = own.astype(BF16)

    pl.semaphore_wait(barrier, 6)

    def rows_of(xx, cc, half):
        return xbuf.at[pl.ds(pl.multiple_of(32 * tp_of(xx, cc) + 16 * half, 16), 16), :]

    mine = [rows_of(x, c, 0), rows_of(x, c, 1)]
    send(mine[0], mine[0], g_ssem.at[0], g_rsem.at[0], xup)
    send(mine[1], mine[1], g_ssem.at[3], g_rsem.at[3], xdn)
    send(mine[1], mine[1], g_ssem.at[1], g_rsem.at[1], xup)
    send(mine[0], mine[0], g_ssem.at[4], g_rsem.at[4], xdn)
    whole = xbuf.at[pl.ds(own_at, 32), :]
    send(whole, whole, d_ssem.at[0], d_rsem.at[0], partner)

    for copy in copies[2:5]:
        copy.wait()
    wa[:, 384:512] = wq[:, 0:128]
    wb[:, 0:128] = jnp.concatenate([wq[:, 128:192], wrk[...]], axis=1)
    wb[:, 128:256] = jnp.concatenate([wlat[...], jnp.zeros((D, 64), BF16)], axis=1)

    order = [
        (0, chip(-1), 0), (3, chip(1), 1), (1, chip(-1), 1), (4, chip(1), 0),
        (2, chip(2), 0), (5, chip(2), 1),
    ]
    for k, (sem, xx, half) in enumerate(order):
        piece = rows_of(xx, c, half)
        arrived(piece, g_rsem.at[sem])
        if sem == 0:
            send(piece, piece, g_ssem.at[2], g_rsem.at[2], xup)
        if sem == 3:
            send(piece, piece, g_ssem.at[5], g_rsem.at[5], xdn)
        send(piece, piece, d_ssem.at[1 + k], d_rsem.at[1 + k], partner)
    theirs = xbuf.at[pl.ds(pl.multiple_of(32 * tp_of(x, 1 - c), 32), 32), :]
    arrived(theirs, d_rsem.at[0])
    for k, (_, xx, half) in enumerate(order):
        arrived(rows_of(xx, 1 - c, half), d_rsem.at[1 + k])

    pb = dot(xbuf[...], wb[...]).astype(BF16)
    lat = pb[:, 128:192]
    latbuf[t] = jnp.concatenate([lat[0:128], lat[128:256]], axis=1)
    for k, peer in enumerate((xup, xfar, xdn)):
        send(latbuf.at[t], latbuf.at[t], l_ssem.at[k], l_rsem.at[k], peer)
    send(latbuf.at[t], latbuf.at[t], ld_ssem.at[0], ld_rsem.at[0], partner)

    for copy in copies[5:]:
        copy.wait()
    signal = dot(xbuf[...], wa[:, 0:256])
    recur = signal[:, 0:128].astype(BF16)
    halo_tx[...] = recur[240:256]
    send(halo_tx, halo_rx, h_sem.at[0], h_sem.at[1], zup)
    gate_s[...] = silu(signal[:, 128:256].astype(BF16).astype(F32))
    rest = dot(xbuf[...], wa[:, 256:512])
    agate_s[...] = silu(rest[:, 0:128].astype(BF16).astype(F32))

    far_row = far[pl.ds(z, 1), :]
    ca, sa, cb, sb = base[:, 0:128], base[:, 128:256], far_row[:, 0:128], far_row[:, 128:256]
    cosine, sine = ca * cb - sa * sb, sa * cb + ca * sb
    lane = lax.broadcasted_iota(jnp.int32, (TOK, 128), 1)
    first = lax.rem(lane, 64) < 32

    def rotated(v):
        swapped = jnp.where(first, -pltpu.roll(v, 96, 1), pltpu.roll(v, 32, 1))
        return v * cosine + swapped * sine

    q_nope = rest[:, 128:256].astype(BF16).astype(F32)
    qr_rk = pb[:, 0:128].astype(F32)
    q_half = jnp.where(lane < 64, qr_rk, 0.0)
    square = jnp.sum(q_nope * q_nope, axis=1, keepdims=True) + jnp.sum(
        q_half * q_half, axis=1, keepdims=True
    )
    scale = lax.rsqrt(square * (1.0 / 192.0) + EPS)
    qgain_rope = jnp.concatenate([qgain[:, 128:192], jnp.ones((1, 64), F32)], axis=1)
    q_nope = q_nope * scale * qgain[:, 0:128]
    turned = rotated(qr_rk * jnp.where(lane < 64, scale * qgain_rope, 1.0))
    zero64 = jnp.zeros((64, TOK), BF16)
    qn_s[...] = jnp.transpose(q_nope).astype(BF16)
    q_rope_t = jnp.transpose(turned)[0:64].astype(BF16)
    qlo_s[...] = jnp.concatenate([q_rope_t, zero64], axis=0)
    qhi_s[...] = jnp.concatenate([zero64, q_rope_t], axis=0)
    key_rope = turned[:, 64:128].astype(BF16)

    for k, o in enumerate((-1, -2, -3)):
        slot = latbuf.at[tp_of(chip(o), c)]
        arrived(slot, l_rsem.at[k])
        send(slot, slot, ld_ssem.at[1 + k], ld_rsem.at[1 + k], partner)
    arrived(latbuf.at[tp_of(x, 1 - c)], ld_rsem.at[0])
    for k, o in enumerate((-1, -2, -3)):
        arrived(latbuf.at[tp_of(chip(o), 1 - c)], ld_rsem.at[1 + k])
    packed = [latbuf[g] for g in range(8)]
    top = jnp.concatenate([v[:, 0:64] for v in packed], axis=1)
    bottom = jnp.concatenate([v[:, 64:128] for v in packed], axis=1)
    latent = jnp.concatenate([top, bottom], axis=0).astype(F32)
    latent = latent * lax.rsqrt(jnp.mean(latent * latent, axis=1, keepdims=True) + EPS) * lgain[...]
    kv = dot(latent.astype(BF16), lup[...])
    k_nope = kv[:, 0:128].astype(BF16)
    v_t = jnp.transpose(kv[:, 128:256]).astype(BF16)
    for h in range(2):
        r, p0 = 320 * h, 128 * h
        kvbuf[z, r : r + 128, :] = k_nope[p0 : p0 + 128]
        kvbuf[z, r + 128 : r + 256, :] = v_t[:, p0 : p0 + 128]
        kvbuf[z, r + 256 : r + 320, :] = jnp.concatenate(
            [key_rope[p0 : p0 + 64], key_rope[p0 + 64 : p0 + 128]], axis=1
        )

    def piece_at(slot, p):
        return kvbuf.at[slot, pl.ds(ROWS * p, ROWS), :]

    def forward(step, slot, direction, p):
        remote(
            piece_at(slot, p), piece_at(slot, p), kv_ssem.at[direction, step, p],
            kv_rsem.at[direction, step, p], zup if direction == 0 else zdn,
        ).start()

    def carry_on(step, slot, direction):
        remote(
            cbuf.at[slot], cbuf.at[slot], c_ssem.at[direction, step],
            c_rsem.at[direction, step], zup if direction == 0 else zdn,
        ).start()

    for p in range(PIECES):
        forward(0, z, 0, p)
        forward(0, z, 1, PIECES - 1 - p)

    row = lax.broadcasted_iota(jnp.int32, (TOK, 128), 0)
    arrived(halo_rx, h_sem.at[1])
    behind = jnp.where(z > 0, halo_rx[...].astype(F32), 0.0)
    recur = recur.astype(F32)
    conv_sum = None
    for tap in range(4):
        back = 3 - tap
        if back:
            moved = pltpu.roll(recur, back, 0)
            edge = pltpu.roll(behind, back, 0)
            edge = jnp.concatenate([edge[0:8], moved[8:TOK]], axis=0)
            term = jnp.where(row < back, edge, moved)
        else:
            term = recur
        term = conv[tap : tap + 1, :] * term
        conv_sum = term if conv_sum is None else conv_sum + term
    conv_out = conv_sum.astype(BF16)
    zb = jnp.zeros((64, 64), BF16)

    def diagonal(w):
        return jnp.concatenate(
            [jnp.concatenate([w[0], zb], axis=1), jnp.concatenate([zb, w[1]], axis=1)], axis=0
        )

    recur_rate = jax.nn.sigmoid(dot(conv_out, diagonal(rblk)))
    input_rate = jax.nn.sigmoid(dot(conv_out, diagonal(iblk)))
    shift = jnp.concatenate(
        [
            jnp.transpose(jnp.broadcast_to(dshift[:, p0 : p0 + 128], (128, 128)))
            for p0 in (0, 128)
        ],
        axis=0,
    )
    log_decay = -8.0 * recur_rate * drate[...] + shift
    a = jnp.exp(log_decay)
    b = jnp.sqrt(minus_expm1(2.0 * log_decay)) * input_rate * conv_out.astype(F32)
    for back in (1, 2, 4, 8, 16, 32, 64, 128):
        inside = row >= back
        a_before = jnp.where(inside, pltpu.roll(a, back, 0), 1.0)
        b_before = jnp.where(inside, pltpu.roll(b, back, 0), 0.0)
        b = a * b_before + b
        a = a * a_before
    a_s[...] = a
    b_s[...] = b
    cbuf[z] = jnp.concatenate([a[TOK - 1 : TOK], b[TOK - 1 : TOK], jnp.zeros((6, 128), F32)], axis=0)
    carry_on(0, z, 0)
    carry_on(0, z, 1)

    to_exp2 = float(192 ** -0.5 * np.log2(np.e))

    def scores(slot, h):
        r = 320 * h
        rope = kvbuf[slot, r + 256 : r + 320, :]
        s = dot(kvbuf[slot, r : r + 128, :], qn_s[...])
        s = s + jnp.concatenate([dot(rope, qlo_s[...]), dot(rope, qhi_s[...])], axis=0)
        return s * to_exp2

    def values(slot, h, weights):
        r = 320 * h
        return dot(kvbuf[slot, r + 128 : r + 256, :], weights.astype(BF16))

    key = lax.broadcasted_iota(jnp.int32, (128, TOK), 0)
    query = lax.broadcasted_iota(jnp.int32, (128, TOK), 1)
    s = [jnp.where(key + 128 * h <= query, scores(z, h), -jnp.inf) for h in range(2)]
    m = jnp.maximum(jnp.max(s[0], axis=0, keepdims=True), jnp.max(s[1], axis=0, keepdims=True))
    w = [jnp.exp2(v - m) for v in s]
    ml_s[0:1, :] = m
    ml_s[1:2, :] = jnp.sum(w[0] + w[1], axis=0, keepdims=True)
    acc_s[...] = values(z, 0, w[0]) + values(z, 1, w[1])

    def attend(slot):
        @pl.when(slot < z)
        def _():
            s = [scores(slot, h) for h in range(2)]
            old = ml_s[0:1, :]
            m = jnp.maximum(old, jnp.max(jnp.maximum(s[0], s[1]), axis=0, keepdims=True))
            w = [jnp.exp2(v - m) for v in s]
            rescale = jnp.exp2(old - m)
            ml_s[0:1, :] = m
            ml_s[1:2, :] = ml_s[1:2, :] * rescale + jnp.sum(w[0] + w[1], axis=0, keepdims=True)
            acc_s[...] = acc_s[...] * rescale + (values(slot, 0, w[0]) + values(slot, 1, w[1]))

    def step(s, up_pieces, dn_pieces, carries, before):
        up, dn = zat(-s), zat(s)
        for k in range(PIECES):
            p, q = k, PIECES - 1 - k
            arrived(piece_at(up, p), kv_rsem.at[0, s - 1, p])
            if p in up_pieces:
                forward(s, up, 0, p)
            arrived(piece_at(dn, q), kv_rsem.at[1, s - 1, q])
            if q in dn_pieces:
                forward(s, dn, 1, q)
            if before and k == 0:
                attend(zat(1 - s))
            if before and k == 1:
                attend(zat(s - 1))
        arrived(cbuf.at[up], c_rsem.at[0, s - 1])
        carry_on(s, up, 0)
        arrived(cbuf.at[dn], c_rsem.at[1, s - 1])
        if carries:
            carry_on(s, dn, 1)

    every = range(PIECES)
    step(1, every, every, True, False)

    def middle(s, _):
        step(s, every, every, True, True)
        return 0

    lax.fori_loop(2, 7, middle, 0)
    step(7, (0, 1), (2, 3), False, True)
    attend(zat(-7))
    attend(zat(7))
    last = zat(8)
    for p in (0, 1):
        arrived(piece_at(last, p), kv_rsem.at[0, 7, p])
        arrived(piece_at(last, 3 - p), kv_rsem.at[1, 7, 3 - p])
    arrived(cbuf.at[last], c_rsem.at[0, 7])
    attend(last)

    def onward(j, state):
        return jnp.where(j < z, cbuf[j, 0:1, :] * state + cbuf[j, 1:2, :], state)

    incoming = lax.fori_loop(0, NZ, onward, init[...])
    xrow[:, 0:128] = ((b_s[...] + a_s[...] * incoming) * gate_s[...]).astype(BF16)
    attended = jnp.transpose(acc_s[...] / ml_s[1:2, :])
    xrow[:, 128:256] = (attended * agate_s[...]).astype(BF16)

    offsets = (2, 1, -1, 0)
    for side, cc in enumerate((1 - c, c)):
        for k, o in enumerate(offsets):
            at = pl.multiple_of(32 * tp_of(chip(o), cc), 32)
            xcat[side, 32 * k : 32 * k + 32, :] = xrow[pl.ds(at, 32), :]
    d2d_tx[...] = dot(xcat[0], wo[...]).astype(BF16)
    for k in range(4):
        part = pl.ds(32 * k, 32)
        send(d2d_tx.at[part, :], d2d_rx.at[part, :], o_ssem.at[k], o_rsem.at[k], partner)
    psum[...] = dot(xcat[1], wo[...])

    def summed(k):
        part = slice(32 * k, 32 * k + 32)
        arrived(d2d_rx.at[pl.ds(32 * k, 32), :], o_rsem.at[k])
        return psum[part, :] + d2d_rx[part, :].astype(F32)

    def reduce_send(k, value, to):
        rtx[k] = value.astype(BF16)
        send(rtx.at[k], rrx.at[k], r_ssem.at[k], r_rsem.at[k], to)

    two = summed(0)
    reduce_send(0, two[:, 0:1024], xup)
    reduce_send(3, two[:, 1024:2048], xdn)
    above = summed(1)
    reduce_send(1, above[:, 1024:2048], xup)
    below = summed(2)
    reduce_send(4, below[:, 0:1024], xdn)
    arrived(rrx.at[0], r_rsem.at[0])
    reduce_send(2, above[:, 0:1024] + rrx[0].astype(F32), xup)
    arrived(rrx.at[3], r_rsem.at[3])
    reduce_send(5, below[:, 1024:2048] + rrx[3].astype(F32), xdn)
    here = summed(3)
    arrived(rrx.at[1], r_rsem.at[1])
    arrived(rrx.at[4], r_rsem.at[4])
    arrived(rrx.at[2], r_rsem.at[2])
    out_ref[:, 0:1024] = (
        here[:, 0:1024] + rrx[4].astype(F32) + rrx[2].astype(F32)
    ).astype(BF16)
    arrived(rrx.at[5], r_rsem.at[5])
    out_ref[:, 1024:2048] = (
        here[:, 1024:2048] + rrx[1].astype(F32) + rrx[5].astype(F32)
    ).astype(BF16)

    for copy in started:
        copy.wait_send()

    def drain(s, _):
        for direction in range(2):
            slot = zat(-s) if direction == 0 else zat(s)
            for p in range(PIECES):
                remote(
                    piece_at(slot, p), piece_at(slot, p), kv_ssem.at[direction, s, p],
                    kv_rsem.at[direction, s, p], partner,
                ).wait_send()
            remote(
                cbuf.at[slot], cbuf.at[slot], c_ssem.at[direction, s],
                c_rsem.at[direction, s], partner,
            ).wait_send()
        return 0

    lax.fori_loop(0, 7, drain, 0)
    for p in (0, 1):
        for direction, q in ((0, p), (1, 3 - p)):
            slot = zat(-7) if direction == 0 else zat(7)
            remote(
                piece_at(slot, q), piece_at(slot, q), kv_ssem.at[direction, 7, q],
                kv_rsem.at[direction, 7, q], partner,
            ).wait_send()
    remote(
        cbuf.at[zat(-7)], cbuf.at[zat(-7)], c_ssem.at[0, 7], c_rsem.at[0, 7], partner
    ).wait_send()


def body(
    tokens, norm_gain, recurrent_input, recurrent_gate, attention_gate, query_proj, latent_down,
    rope_key_down, conv_kernel, recurrence_gate_blocks, input_gate_blocks, decay_rate,
    decay_shift, initial_state, latent_gain, latent_up, query_gain, recurrent_output,
    attention_output,
):
    base, far = (jnp.asarray(v) for v in rotary_tables())

    def row(v):
        return v.reshape(1, -1)

    operands = (
        tokens, row(norm_gain), recurrent_input, recurrent_gate, attention_gate, query_proj,
        latent_down, rope_key_down, conv_kernel, recurrence_gate_blocks, input_gate_blocks,
        row(decay_rate), row(decay_shift), row(initial_state), row(latent_gain), latent_up,
        row(query_gain), recurrent_output, attention_output, base, far,
    )
    dma, vmem = pltpu.SemaphoreType.DMA, pltpu.VMEM
    scratch = [
        vmem((32, D), BF16), vmem((1, D), F32), vmem((D, 512), BF16), vmem((D, 256), BF16),
        vmem((D, 192), BF16), vmem((D, 64), BF16), vmem((D, 64), BF16), vmem((4, 128), F32),
        vmem((2, 64, 64), BF16), vmem((2, 64, 64), BF16), vmem((1, 128), F32),
        vmem((1, TOK), F32), vmem((1, 128), F32), vmem((1, 512), F32), vmem((512, 256), BF16),
        vmem((1, 192), F32), vmem((256, D), BF16), vmem((TOK, 256), F32), vmem((NZ, 256), F32),
        vmem((TOK, D), BF16), vmem((8, 128, 128), BF16), vmem((16, 128), BF16),
        vmem((16, 128), BF16), vmem((NZ, PIECES * ROWS, 128), BF16), vmem((NZ, 8, 128), F32),
        vmem((128, TOK), BF16), vmem((128, TOK), BF16), vmem((128, TOK), BF16),
        vmem((128, TOK), F32), vmem((8, TOK), F32), vmem((TOK, 128), F32),
        vmem((TOK, 128), F32), vmem((TOK, 128), F32), vmem((TOK, 128), F32),
        vmem((TOK, 256), BF16), vmem((2, 128, 256), BF16), vmem((128, D), BF16),
        vmem((128, D), BF16), vmem((128, D), F32), vmem((6, 32, 1024), BF16),
        vmem((6, 32, 1024), BF16),
        dma((len(operands),)), dma((6,)), dma((6,)), dma((7,)), dma((7,)), dma((3,)), dma((3,)),
        dma((4,)), dma((4,)), dma((2,)), dma((2, 8, PIECES)), dma((2, 8, PIECES)), dma((2, 8)),
        dma((2, 8)), dma((4,)), dma((4,)), dma((6,)), dma((6,)),
    ]
    return pl.pallas_call(
        kernel,
        out_shape=jax.ShapeDtypeStruct((32, D), BF16),
        in_specs=[pl.BlockSpec(memory_space=pl.ANY)] * len(operands),
        out_specs=pl.BlockSpec(memory_space=pltpu.VMEM),
        scratch_shapes=scratch,
        compiler_params=pltpu.CompilerParams(
            collective_id=0, has_side_effects=True, vmem_limit_bytes=56 * 2**20
        ),
    )(*operands)


def solution(mesh):
    return jax.shard_map(
        body,
        mesh=mesh,
        in_specs=(
            P(("fs", "sp", "tp"), None), P(), P(None, "tp"), P(None, "tp"), P(None, "tp"),
            P(None, "tp"), P(None, "tp"), P(), P(None, "tp"), P("tp", None, None),
            P("tp", None, None), P("tp"), P(("fs", "sp")), P(("fs", "tp")), P(), P(None, "tp"),
            P(), P("tp", None), P("tp", None),
        ),
        out_specs=P(("fs", "sp", "tp"), None),
        check_vma=False,
    )
```

time: 202 us -> 76.6 us (0.38); the launches traced: 198 us -> 76.5 us
  Pallas kernels: 0 us -> 70.5 us
  local copies, waits for them, and re-layouts: 64.1 us -> 5.92 us
  waiting for transfers between devices: 32.6 us -> 0 us
  blocking collectives: 31.2 us -> 0 us
  starting transfers between devices: 28 us -> 0 us
  matrix products: 18.3 us -> 0 us
  between operations: 14.8 us -> 0.01 us
  other arithmetic: 8.94 us -> 0 us
    pallas_call x0 -> x1, Pallas kernels: none -> 70.5 us  [body(): pl.pallas_call(kernel, out_shape=jax.ShapeDtypeStruct((32, D), BF16), in_...]
    all_to_all x1 -> x0, blocking collectives: 31.2 us -> none  [summed_on_arrival(): lax.all_to_all(in_blocks(shard, dim, count), axis, 0, 0, tiled=True)]
    slice x60 -> x0, local copies, waits for them, and re-layouts: 30.2 us -> none  [the longest x42 28.2 us: body(): lax.associative_scan(linear_step, (decay, driven), axis=0)]
    all_to_all x3 -> x0, starting transfers between devices: 26.6 us -> none  [copy_for_each(): return lax.all_to_all(copies, axis, split_axis=0, concat_axis=0, tiled=True)]
    pad x28 -> x0, local copies, waits for them, and re-layouts: 19.2 us -> none  [body(): lax.associative_scan(linear_step, (decay, driven), axis=0)]
    dot_general x18 -> x0, matrix products: 18.3 us -> none  [the longest x4 5.13 us: online_step(): jnp.einsum('htk,khd->thd', weights.astype(jnp.bfloat16), value_block, pre...]
    all_gather x1 -> x0, waiting for transfers between devices: 16.6 us -> none  [sent_together(): lax.all_gather(both, axis, axis=dim, tiled=True)]
    all_to_all x3 -> x0, waiting for transfers between devices: 16 us -> none  [copy_for_each(): return lax.all_to_all(copies, axis, split_axis=0, concat_axis=0, tiled=True)]
  transfers between devices with their start and end apart: 5 -> 0, of which waited for: 3 -> 0; matrix products, arithmetic and copies ran while one was open for 33% -> 0% of each run, Pallas kernels for 0% -> 0%
where the time goes in v1:
time: 76.6 us; the launch traced here: 76.5 us
  Pallas kernels  70.5 us (92%)
  local copies, waits for them, and re-layouts  5.92 us (8%)
    pallas_call x1, Pallas kernels, body(): pl.pallas_call(kernel, out_shape=jax.ShapeDtypeStruct((32, D), BF16), in_...  70.5 us
    unnamed x8, local copies, waits for them, and re-layouts  5.92 us

profile of v1, /device:TPU:1, one launch (start us, length us, event | category | flops | bytes accessed | tf_op | source)
XLA Modules:
  0.0 76.5 jit_solution(11523712131536297979)
XLA Ops:
  0.0 0.0 copy-start.1
  0.0 0.0 copy-start
  0.0 2.1 %copy.23.wlat_h = bf16[2048,64]{1,0:T(8,128)(2,1)} copy(bf16[2048,64]{0,1:T(8,128)(2,1)} %param.27) | data formatting | bytes 524288 | tf_op args[6]
  2.1 0.0 copy-done.1
  2.1 1.0 %copy.24.wrk_h = bf16[2048,64]{1,0:T(8,128)(2,1)} copy(bf16[2048,64]{0,1:T(8,128)(2,1)S(1)} %copy-done.1) | data formatting | bytes 524288 | tf_op args[7]
  3.1 0.0 copy-done
  3.1 1.3 %copy.22.wq_h = bf16[2048,192]{1,0:T(8,128)(2,1)} copy(bf16[2048,192]{0,1:T(8,128)(2,1)S(1)} %copy-done) | data formatting | bytes 1572864 | tf_op args[5]
  4.4 70.5 %shard_map.199 = bf16[32,2048]{1,0:T(8,128)(2,1)} custom-call(bf16[32,2048]{1,0:T(8,128)(2,1)} %tok_h.1, f32[1,2048]{1,0:T(1,128)} %bitcast.6, bf16[2048,128]{1,0:T(8,128)(2,1)} %rin_h.1, bf16[2048,128]{1,0:T(8,128)(2,1)} %rgate_h.1, bf16[2048,128]{1,0:T(8,128)(2,1)} %agate_h.1, bf16[2048,192]{1,0:T(8,128)(2,1)} %copy.22.wq_h, ...), custom_call_target="tpu_custom_call" | custom-call | tf_op jit(solution)/shard_map/pallas_call | solution.py:470
  74.9 1.6 %copy.26 = bf16[32,2048]{1,0:T(8,128)(2,1)} copy(bf16[32,2048]{1,0:T(8,128)(2,1)} %shard_map.199) | data formatting | bytes 262144
Async XLA Ops:
  0.0 2.1 %copy-start.1 = (bf16[2048,64]{0,1:T(8,128)(2,1)S(1)}, bf16[2048,64]{0,1:T(8,128)(2,1)}, u32[]{:S(2)}) copy-start(bf16[2048,64]{0,1:T(8,128)(2,1)} %param.28) | copy-start | bytes 786436
  0.0 3.1 %copy-start = (bf16[2048,192]{0,1:T(8,128)(2,1)S(1)}, bf16[2048,192]{0,1:T(8,128)(2,1)}, u32[]{:S(2)}) copy-start(bf16[2048,192]{0,1:T(8,128)(2,1)} %param.26) | copy-start | bytes 2359300

commit v2 on v1

--- a/solution.py
+++ b/solution.py
@@ -13,7 +13,8 @@
 THETA = 10000.0
 F32, BF16 = jnp.float32, jnp.bfloat16
 NZ, NX, TOK, D = 16, 4, 256, 2048
-PIECES, ROWS = 4, 160
+PIECES, ROWS = 6, 96
+UP, DOWN = 8, 7
 NT = (((1,), (1,)), ((), ()))
 
 
@@ -47,12 +48,12 @@
     tok_h, ngain_h, rin_h, rgate_h, agate_h, wq_h, wlat_h, wrk_h, conv_h, rblk_h, iblk_h,
     drate_h, dshift_h, init_h, lgain_h, lup_h, qgain_h, rout_h, aout_h, base_h, far_h,
     out_ref,
-    tok, ngain, wa, wb, wq, wlat, wrk, conv, rblk, iblk, drate, dshift, init, lgain, lup,
+    tok, ngain, wa, wb, wt, conv, rblk, iblk, drate, dshift, init, lgain, lup,
     qgain, wo, base, far,
     xbuf, latbuf, halo_tx, halo_rx, kvbuf, cbuf, qn_s, qlo_s, qhi_s, acc_s, ml_s,
     a_s, b_s, gate_s, agate_s, xrow, xcat, d2d_tx, d2d_rx, psum, rtx, rrx,
     in_sem, g_ssem, g_rsem, d_ssem, d_rsem, l_ssem, l_rsem, ld_ssem, ld_rsem, h_sem,
-    kv_ssem, kv_rsem, c_ssem, c_rsem, o_ssem, o_rsem, r_ssem, r_rsem,
+    kv_ssem, kv_rsem, s_ssem, s_rsem, c_ssem, c_rsem, o_ssem, o_rsem, r_ssem, r_rsem,
 ):
     z = lax.axis_index("sp")
     t = lax.axis_index("tp")
@@ -91,7 +92,8 @@
         pl.semaphore_signal(barrier, inc=1, device_id=peer, device_id_type=MESH)
 
     loads = [
-        (tok_h, tok), (ngain_h, ngain), (wq_h, wq), (wlat_h, wlat), (wrk_h, wrk),
+        (tok_h, tok), (ngain_h, ngain), (wq_h, wt.at[0:192]), (wrk_h, wt.at[192:256]),
+        (wlat_h, wt.at[256:320]),
         (rin_h, wa.at[:, 0:128]), (rgate_h, wa.at[:, 128:256]), (agate_h, wa.at[:, 256:384]),
         (conv_h, conv), (rblk_h, rblk), (iblk_h, iblk), (drate_h, drate), (dshift_h, dshift),
         (init_h, init), (lgain_h, lgain), (lup_h, lup), (qgain_h, qgain),
@@ -123,9 +125,9 @@
 
     for copy in copies[2:5]:
         copy.wait()
-    wa[:, 384:512] = wq[:, 0:128]
-    wb[:, 0:128] = jnp.concatenate([wq[:, 128:192], wrk[...]], axis=1)
-    wb[:, 128:256] = jnp.concatenate([wlat[...], jnp.zeros((D, 64), BF16)], axis=1)
+    wa[:, 384:512] = jnp.transpose(wt[0:128])
+    wb[:, 0:128] = jnp.transpose(wt[128:256])
+    wb[:, 128:256] = jnp.transpose(wt[256:384])
 
     order = [
         (0, chip(-1), 0), (3, chip(1), 1), (1, chip(-1), 1), (4, chip(1), 0),
@@ -156,7 +158,8 @@
     signal = dot(xbuf[...], wa[:, 0:256])
     recur = signal[:, 0:128].astype(BF16)
     halo_tx[...] = recur[240:256]
-    send(halo_tx, halo_rx, h_sem.at[0], h_sem.at[1], zup)
+    halo = remote(halo_tx, halo_rx, h_sem.at[0], h_sem.at[1], zup)
+    pl.when(z < NZ - 1)(lambda: halo.start())
     gate_s[...] = silu(signal[:, 128:256].astype(BF16).astype(F32))
     rest = dot(xbuf[...], wa[:, 256:512])
     agate_s[...] = silu(rest[:, 0:128].astype(BF16).astype(F32))
@@ -204,20 +207,21 @@
     k_nope = kv[:, 0:128].astype(BF16)
     v_t = jnp.transpose(kv[:, 128:256]).astype(BF16)
     for h in range(2):
-        r, p0 = 320 * h, 128 * h
+        r, p0 = 64 + 256 * h, 128 * h
         kvbuf[z, r : r + 128, :] = k_nope[p0 : p0 + 128]
         kvbuf[z, r + 128 : r + 256, :] = v_t[:, p0 : p0 + 128]
-        kvbuf[z, r + 256 : r + 320, :] = jnp.concatenate(
+        kvbuf[z, 576 * h : 576 * h + 64, :] = jnp.concatenate(
             [key_rope[p0 : p0 + 64], key_rope[p0 + 64 : p0 + 128]], axis=1
         )
 
-    def piece_at(slot, p):
-        return kvbuf.at[slot, pl.ds(ROWS * p, ROWS), :]
-
-    def forward(step, slot, direction, p):
+    def piece_at(slot, k):
+        p = k + c * (PIECES - 1 - 2 * k)
+        return kvbuf.at[slot, pl.ds(pl.multiple_of(64 * c + ROWS * p, 16), ROWS), :]
+
+    def forward(step, slot, direction, k):
         remote(
-            piece_at(slot, p), piece_at(slot, p), kv_ssem.at[direction, step, p],
-            kv_rsem.at[direction, step, p], zup if direction == 0 else zdn,
+            piece_at(slot, k), piece_at(slot, k), kv_ssem.at[direction, step],
+            kv_rsem.at[direction, step, k], zup if direction == 0 else zdn,
         ).start()
 
     def carry_on(step, slot, direction):
@@ -226,12 +230,22 @@
             c_rsem.at[direction, step], zup if direction == 0 else zdn,
         ).start()
 
-    for p in range(PIECES):
-        forward(0, z, 0, p)
-        forward(0, z, 1, PIECES - 1 - p)
+    def shared(slot, core):
+        return kvbuf.at[slot, pl.ds(pl.multiple_of(576 * core, 64), 64), :]
+
+    def share(step, slot, direction):
+        return remote(
+            shared(slot, c), shared(slot, c), s_ssem.at[direction, step],
+            s_rsem.at[direction, step], partner,
+        )
+
+    sends_up, sends_dn = z < NZ - 1, z < DOWN
+    for k in range(PIECES):
+        pl.when(sends_up)(lambda: forward(0, z, 0, k))
+        pl.when(sends_dn)(lambda: forward(0, z, 1, k))
 
     row = lax.broadcasted_iota(jnp.int32, (TOK, 128), 0)
-    arrived(halo_rx, h_sem.at[1])
+    pl.when(z > 0)(lambda: arrived(halo_rx, h_sem.at[1]))
     behind = jnp.where(z > 0, halo_rx[...].astype(F32), 0.0)
     recur = recur.astype(F32)
     conv_sum = None
@@ -275,20 +289,20 @@
     a_s[...] = a
     b_s[...] = b
     cbuf[z] = jnp.concatenate([a[TOK - 1 : TOK], b[TOK - 1 : TOK], jnp.zeros((6, 128), F32)], axis=0)
-    carry_on(0, z, 0)
-    carry_on(0, z, 1)
+    pl.when(sends_up)(lambda: carry_on(0, z, 0))
+    pl.when(sends_dn)(lambda: carry_on(0, z, 1))
 
     to_exp2 = float(192 ** -0.5 * np.log2(np.e))
 
     def scores(slot, h):
-        r = 320 * h
-        rope = kvbuf[slot, r + 256 : r + 320, :]
+        r = 64 + 256 * h
+        rope = kvbuf[slot, 576 * h : 576 * h + 64, :]
         s = dot(kvbuf[slot, r : r + 128, :], qn_s[...])
         s = s + jnp.concatenate([dot(rope, qlo_s[...]), dot(rope, qhi_s[...])], axis=0)
         return s * to_exp2
 
     def values(slot, h, weights):
-        r = 320 * h
+        r = 64 + 256 * h
         return dot(kvbuf[slot, r + 128 : r + 256, :], weights.astype(BF16))
 
     key = lax.broadcasted_iota(jnp.int32, (128, TOK), 0)
@@ -300,9 +314,10 @@
     ml_s[1:2, :] = jnp.sum(w[0] + w[1], axis=0, keepdims=True)
     acc_s[...] = values(z, 0, w[0]) + values(z, 1, w[1])
 
-    def attend(slot):
+    def attend(step, slot, direction):
         @pl.when(slot < z)
         def _():
+            arrived(shared(slot, 1 - c), s_rsem.at[direction, step])
             s = [scores(slot, h) for h in range(2)]
             old = ml_s[0:1, :]
             m = jnp.maximum(old, jnp.max(jnp.maximum(s[0], s[1]), axis=0, keepdims=True))
@@ -312,43 +327,65 @@
             ml_s[1:2, :] = ml_s[1:2, :] * rescale + jnp.sum(w[0] + w[1], axis=0, keepdims=True)
             acc_s[...] = acc_s[...] * rescale + (values(slot, 0, w[0]) + values(slot, 1, w[1]))
 
-    def step(s, up_pieces, dn_pieces, carries, before):
-        up, dn = zat(-s), zat(s)
+    def came_up(s):
+        return zat(-s), s <= z
+
+    def came_down(s):
+        slot = zat(s)
+        return slot, slot < DOWN
+
+    def step(s, down, onward, before):
+        up, has_up = came_up(s)
+        dn, has_dn = came_down(s)
         for k in range(PIECES):
-            p, q = k, PIECES - 1 - k
-            arrived(piece_at(up, p), kv_rsem.at[0, s - 1, p])
-            if p in up_pieces:
-                forward(s, up, 0, p)
-            arrived(piece_at(dn, q), kv_rsem.at[1, s - 1, q])
-            if q in dn_pieces:
-                forward(s, dn, 1, q)
-            if before and k == 0:
-                attend(zat(1 - s))
+
+            @pl.when(has_up)
+            def _():
+                arrived(piece_at(up, k), kv_rsem.at[0, s - 1, k])
+                if onward:
+                    pl.when(sends_up)(lambda: forward(s, up, 0, k))
+                if k == 0:
+                    share(s - 1, up, 0).start()
+
+            if down:
+
+                @pl.when(has_dn)
+                def _():
+                    arrived(piece_at(dn, k), kv_rsem.at[1, s - 1, k])
+                    if onward and down != "last":
+                        forward(s, dn, 1, k)
+                    if k == 0:
+                        pl.when(dn < z)(lambda: share(s - 1, dn, 1).start())
+
             if before and k == 1:
-                attend(zat(s - 1))
-        arrived(cbuf.at[up], c_rsem.at[0, s - 1])
-        carry_on(s, up, 0)
-        arrived(cbuf.at[dn], c_rsem.at[1, s - 1])
-        if carries:
-            carry_on(s, dn, 1)
-
-    every = range(PIECES)
-    step(1, every, every, True, False)
+                attend(s - 2, zat(1 - s), 0)
+            if before and k == 3:
+                attend(s - 2, zat(s - 1), 1)
+
+        @pl.when(has_up)
+        def _():
+            arrived(cbuf.at[up], c_rsem.at[0, s - 1])
+            if onward:
+                pl.when(sends_up)(lambda: carry_on(s, up, 0))
+
+        if down:
+
+            @pl.when(has_dn)
+            def _():
+                arrived(cbuf.at[dn], c_rsem.at[1, s - 1])
+                if onward and down != "last":
+                    carry_on(s, dn, 1)
+
+    step(1, True, True, False)
 
     def middle(s, _):
-        step(s, every, every, True, True)
+        step(s, True, True, True)
         return 0
 
-    lax.fori_loop(2, 7, middle, 0)
-    step(7, (0, 1), (2, 3), False, True)
-    attend(zat(-7))
-    attend(zat(7))
-    last = zat(8)
-    for p in (0, 1):
-        arrived(piece_at(last, p), kv_rsem.at[0, 7, p])
-        arrived(piece_at(last, 3 - p), kv_rsem.at[1, 7, 3 - p])
-    arrived(cbuf.at[last], c_rsem.at[0, 7])
-    attend(last)
+    lax.fori_loop(2, DOWN, middle, 0)
+    step(DOWN, "last", True, True)
+    step(UP, False, False, True)
+    attend(UP - 1, zat(-UP), 0)
 
     def onward(j, state):
         return jnp.where(j < z, cbuf[j, 0:1, :] * state + cbuf[j, 1:2, :], state)
@@ -404,31 +441,36 @@
     for copy in started:
         copy.wait_send()
 
+    pl.when(z < NZ - 1)(lambda: halo.wait_send())
+
     def drain(s, _):
-        for direction in range(2):
-            slot = zat(-s) if direction == 0 else zat(s)
-            for p in range(PIECES):
+        for direction, (slot, has) in ((0, came_up(s)), (1, came_down(s))):
+            goes = has & (sends_up if direction == 0 else s < DOWN)
+            mine = kvbuf.at[slot, pl.ds(0, PIECES * ROWS), :]
+
+            @pl.when(goes)
+            def _():
                 remote(
-                    piece_at(slot, p), piece_at(slot, p), kv_ssem.at[direction, s, p],
-                    kv_rsem.at[direction, s, p], partner,
+                    mine, mine, kv_ssem.at[direction, s], kv_rsem.at[direction, s, 0], partner
                 ).wait_send()
-            remote(
-                cbuf.at[slot], cbuf.at[slot], c_ssem.at[direction, s],
-                c_rsem.at[direction, s], partner,
-            ).wait_send()
+                remote(
+                    cbuf.at[slot], cbuf.at[slot], c_ssem.at[direction, s],
+                    c_rsem.at[direction, s], partner,
+                ).wait_send()
+
         return 0
 
-    lax.fori_loop(0, 7, drain, 0)
-    for p in (0, 1):
-        for direction, q in ((0, p), (1, 3 - p)):
-            slot = zat(-7) if direction == 0 else zat(7)
-            remote(
-                piece_at(slot, q), piece_at(slot, q), kv_ssem.at[direction, 7, q],
-                kv_rsem.at[direction, 7, q], partner,
-            ).wait_send()
-    remote(
-        cbuf.at[zat(-7)], cbuf.at[zat(-7)], c_ssem.at[0, 7], c_rsem.at[0, 7], partner
-    ).wait_send()
+    lax.fori_loop(0, UP, drain, 0)
+
+    def drain_shared(s, _):
+        for direction, slot in ((0, zat(-1 - s)), (1, zat(1 + s))):
+            if direction == 0:
+                pl.when(slot < z)(lambda: share(s, slot, 0).wait_send())
+            else:
+                pl.when((slot < z) & (s < DOWN))(lambda: share(s, slot, 1).wait_send())
+        return 0
+
+    lax.fori_loop(0, UP, drain_shared, 0)
 
 
 def body(
@@ -443,20 +485,20 @@
         return v.reshape(1, -1)
 
     operands = (
-        tokens, row(norm_gain), recurrent_input, recurrent_gate, attention_gate, query_proj,
-        latent_down, rope_key_down, conv_kernel, recurrence_gate_blocks, input_gate_blocks,
+        tokens, row(norm_gain), recurrent_input, recurrent_gate, attention_gate, query_proj.T,
+        latent_down.T, rope_key_down.T, conv_kernel, recurrence_gate_blocks, input_gate_blocks,
         row(decay_rate), row(decay_shift), row(initial_state), row(latent_gain), latent_up,
         row(query_gain), recurrent_output, attention_output, base, far,
     )
     dma, vmem = pltpu.SemaphoreType.DMA, pltpu.VMEM
     scratch = [
         vmem((32, D), BF16), vmem((1, D), F32), vmem((D, 512), BF16), vmem((D, 256), BF16),
-        vmem((D, 192), BF16), vmem((D, 64), BF16), vmem((D, 64), BF16), vmem((4, 128), F32),
+        vmem((384, D), BF16), vmem((4, 128), F32),
         vmem((2, 64, 64), BF16), vmem((2, 64, 64), BF16), vmem((1, 128), F32),
         vmem((1, TOK), F32), vmem((1, 128), F32), vmem((1, 512), F32), vmem((512, 256), BF16),
         vmem((1, 192), F32), vmem((256, D), BF16), vmem((TOK, 256), F32), vmem((NZ, 256), F32),
         vmem((TOK, D), BF16), vmem((8, 128, 128), BF16), vmem((16, 128), BF16),
-        vmem((16, 128), BF16), vmem((NZ, PIECES * ROWS, 128), BF16), vmem((NZ, 8, 128), F32),
+        vmem((16, 128), BF16), vmem((NZ, 640, 128), BF16), vmem((NZ, 8, 128), F32),
         vmem((128, TOK), BF16), vmem((128, TOK), BF16), vmem((128, TOK), BF16),
         vmem((128, TOK), F32), vmem((8, TOK), F32), vmem((TOK, 128), F32),
         vmem((TOK, 128), F32), vmem((TOK, 128), F32), vmem((TOK, 128), F32),
@@ -464,7 +506,7 @@
         vmem((128, D), BF16), vmem((128, D), F32), vmem((6, 32, 1024), BF16),
         vmem((6, 32, 1024), BF16),
         dma((len(operands),)), dma((6,)), dma((6,)), dma((7,)), dma((7,)), dma((3,)), dma((3,)),
-        dma((4,)), dma((4,)), dma((2,)), dma((2, 8, PIECES)), dma((2, 8, PIECES)), dma((2, 8)),
+        dma((4,)), dma((4,)), dma((2,)), dma((2, 8)), dma((2, 8, PIECES)), dma((2, 8)), dma((2, 8)), dma((2, 8)),
         dma((2, 8)), dma((4,)), dma((4,)), dma((6,)), dma((6,)),
     ]
     return pl.pallas_call(

time: 76.6 us -> 62.3 us (0.81)
  the two profiles are of different devices: /device:TPU:1 before, /device:TPU:408 now
where the time goes in v2:
time: 62.3 us; the launch traced here: 61.9 us
  Pallas kernels  60.3 us (97%)
  local copies, waits for them, and re-layouts  1.57 us (3%)
    pallas_call x1, Pallas kernels, body(): pl.pallas_call(kernel, out_shape=jax.ShapeDtypeStruct((32, D), BF16), in_...  60.3 us
    unnamed x1, local copies, waits for them, and re-layouts  1.57 us

profile of v2, /device:TPU:408, one launch (start us, length us, event | category | flops | bytes accessed | tf_op | source)
XLA Modules:
  0.0 61.9 jit_solution(2828035597445155114)
XLA Ops:
  0.0 60.3 %shard_map.199 = bf16[32,2048]{1,0:T(8,128)(2,1)} custom-call(bf16[32,2048]{1,0:T(8,128)(2,1)} %tok_h.1, f32[1,2048]{1,0:T(1,128)} %bitcast.12, bf16[2048,128]{1,0:T(8,128)(2,1)} %rin_h.1, bf16[2048,128]{1,0:T(8,128)(2,1)} %rgate_h.1, bf16[2048,128]{1,0:T(8,128)(2,1)} %agate_h.1, bf16[192,2048]{1,0:T(8,128)(2,1)} %bitcast.9, bf16[64,2048]{1,0:T(8,128)(2,1)} %bitcast.10, ...), custom_call_target="tpu_custom_call" | custom-call | tf_op jit(solution)/shard_map/pallas_call | solution.py:512
  60.4 1.6 %copy.23 = bf16[32,2048]{1,0:T(8,128)(2,1)} copy(bf16[32,2048]{1,0:T(8,128)(2,1)} %shard_map.199) | data formatting | bytes 262144

commit v3 on v2

v3 whole, which is shorter than its diff:
```python
import functools

import jax
import jax.numpy as jnp
import numpy as np
from jax import lax
from jax.experimental import pallas as pl
from jax.experimental.pallas import tpu as pltpu
from jax.sharding import PartitionSpec as P

MESH = pl.DeviceIdType.MESH
EPS = 1e-06
THETA = 10000.0
F32, BF16 = jnp.float32, jnp.bfloat16
NZ, NX, TOK, D = 16, 4, 256, 2048
PIECES, HALF, ROWS = 6, 3, 96
UP, DOWN = 8, 7
NT = (((1,), (1,)), ((), ()))


def dot(a, b):
    return jnp.dot(a, b, preferred_element_type=F32)


def silu(v):
    return v * jax.nn.sigmoid(v)


def minus_expm1(y):
    series = 1.0 + y * (1.0 / 8.0)
    for n in (7, 6, 5, 4, 3, 2):
        series = 1.0 + y * (1.0 / n) * series
    return jnp.where(y > -0.35, -y * series, 1.0 - jnp.exp(y))


def rotary_tables():
    inv = 1.0 / THETA ** (np.arange(0, 64, 2, dtype=np.float64) / 64)
    lanes = np.tile(inv, 4)

    def table(positions):
        angles = positions[:, None].astype(np.float64) * lanes[None]
        return np.concatenate([np.cos(angles), np.sin(angles)], 1).astype(np.float32)

    return table(np.arange(TOK)), table(TOK * np.arange(NZ))


def kernel(
    tok_h, ngain_h, rin_h, rgate_h, agate_h, wq_h, wlat_h, wrk_h, conv_h, rblk_h, iblk_h,
    drate_h, dshift_h, init_h, lgain_h, lup_h, qgain_h, rout_h, aout_h, base_h, far_h,
    out_ref,
    tok, ngain, wa, wb, wt, conv, blocks, small, lup, qgain, wo, tables,
    xbuf, pbuf, latbuf, halo_tx, halo_rx, kvbuf, cbuf, qn_s, qlo_s, qhi_s, acc_s, ml_s,
    a_s, b_s, gate_s, agate_s, xrow, xcat, d2d_tx, d2d_rx, psum, rtx, rrx,
    in_sem, x_ssem, up_rsem, dn_rsem, d_rsem, l_ssem, l_rsem, ld_rsem, h_sem,
    up_ssem, dn_ssem, upkv_rsem, dnkv_rsem, s_ssem, s_rsem, c_rsem, o_ssem, o_rsem, r_ssem, r_rsem,
):
    z = lax.axis_index("sp")
    t = lax.axis_index("tp")
    x, c = lax.div(t, 2), lax.rem(t, 2)

    def chip(offset):
        return lax.rem(x + (offset + NX), NX)

    def tp_of(xx, cc):
        return 2 * xx + cc

    def zat(offset):
        return lax.rem(z + (offset + 2 * NZ), NZ)

    partner = {"tp": tp_of(x, 1 - c)}
    xup, xdn, xfar = ({"tp": tp_of(chip(o), c)} for o in (1, -1, 2))
    zup, zdn = {"sp": zat(1)}, {"sp": zat(-1)}
    across = [{"tp": tp_of(chip(o), 1 - c)} for o in (1, -1, 2)]

    def remote(src, dst, ssem, rsem, to):
        return pltpu.make_async_remote_copy(
            src_ref=src, dst_ref=dst, send_sem=ssem, recv_sem=rsem, device_id=to,
            device_id_type=MESH,
        )

    def send(src, dst, ssem, rsem, to):
        remote(src, dst, ssem, rsem, to).start()

    def arrived(dst, rsem):
        remote(dst, dst, rsem, rsem, partner).wait_recv()

    def sent(as_much, ssem):
        remote(as_much, as_much, ssem, ssem, partner).wait_send()

    barrier = pltpu.get_barrier_semaphore()
    for peer in (partner, xup, xdn, xfar, zup, zdn, *across):
        pl.semaphore_signal(barrier, inc=1, device_id=peer, device_id_type=MESH)

    loads = [
        (0, tok, [(tok_h, tok)]),
        (1, ngain, [(ngain_h, ngain)]),
        (2, wt.at[0:320], [(wq_h, wt.at[0:192]), (wrk_h, wt.at[192:256]), (wlat_h, wt.at[256:320])]),
        (3, wa.at[:, 0:384], [
            (rin_h, wa.at[:, 0:128]), (rgate_h, wa.at[:, 128:256]), (agate_h, wa.at[:, 256:384])
        ]),
        (4, conv, [(conv_h, conv)]),
        (5, blocks, [(rblk_h, blocks.at[0:2]), (iblk_h, blocks.at[2:4])]),
        (6, small, [
            (drate_h, small.at[0:1]), (init_h, small.at[1:2]), (dshift_h, small.at[2:4]),
            (lgain_h, small.at[4:8]),
        ]),
        (7, lup, [(lup_h, lup)]),
        (8, qgain, [(qgain_h, qgain)]),
        (9, wo, [(rout_h, wo.at[0:128]), (aout_h, wo.at[128:256])]),
        (10, tables, [(base_h, tables.at[0:TOK]), (far_h, tables.at[TOK : TOK + NZ])]),
    ]
    for k, _, copies in loads:
        for source, target in copies:
            pltpu.make_async_copy(source, target, in_sem.at[k]).start()

    def loaded(k):
        pltpu.make_async_copy(loads[k][1], loads[k][1], in_sem.at[k]).wait()

    loaded(0)
    loaded(1)
    own = tok[...].astype(F32)
    own = own * lax.rsqrt(jnp.mean(own * own, axis=1, keepdims=True) + EPS) * ngain[...]
    own_at = pl.multiple_of(32 * t, 32)
    xbuf[pl.ds(own_at, 32), :] = own.astype(BF16)

    pl.semaphore_wait(barrier, 9)

    def rows_of(xx, cc, half, columns=slice(None)):
        return xbuf.at[pl.ds(pl.multiple_of(32 * tp_of(xx, cc) + 16 * half, 16), 16), columns]

    left, right = slice(0, 1024), slice(1024, 2048)

    for k, part in enumerate((left, right)):
        send(rows_of(x, c, 0, part), rows_of(x, c, 0, part), x_ssem, up_rsem.at[k], xup)
        send(rows_of(x, c, 1, part), rows_of(x, c, 1, part), x_ssem, dn_rsem.at[k], xdn)
    send(rows_of(x, c, 1), rows_of(x, c, 1), x_ssem, up_rsem.at[2], xup)
    send(rows_of(x, c, 0), rows_of(x, c, 0), x_ssem, dn_rsem.at[2], xdn)
    whole = xbuf.at[pl.ds(own_at, 32), :]
    send(whole, whole, x_ssem, d_rsem.at[0], partner)

    loaded(2)
    wa[:, 384:512] = jnp.transpose(wt[0:128])
    wb[:, 0:128] = jnp.transpose(wt[128:256])
    wb[:, 128:256] = jnp.transpose(wt[256:384])

    for k, part in enumerate((left, right)):
        for piece, rsem, to in (
            (rows_of(chip(-1), c, 0, part), up_rsem, xup),
            (rows_of(chip(1), c, 1, part), dn_rsem, xdn),
        ):
            arrived(piece, rsem.at[k])
            send(piece, piece, x_ssem, rsem.at[3 + k], to)
            send(piece, piece, x_ssem, d_rsem.at[0], partner)
    for piece, rsem in ((rows_of(chip(-1), c, 1), up_rsem), (rows_of(chip(1), c, 0), dn_rsem)):
        arrived(piece, rsem.at[2])
        send(piece, piece, x_ssem, d_rsem.at[0], partner)
    arrived(xbuf.at[0:96, :], d_rsem.at[0])

    def segment(o):
        return pl.ds(pl.multiple_of(64 * chip(o), 64), 64)

    def project(offsets):
        rows = jnp.concatenate([xbuf[segment(o), :] for o in offsets], axis=0)
        out = dot(rows, wb[...]).astype(BF16)
        for k, o in enumerate(offsets):
            pbuf[segment(o), :] = out[64 * k : 64 * k + 64, 0:128]
            lat = out[64 * k : 64 * k + 64, 128:192]
            latbuf[t, 32 * o + 32 : 32 * o + 64, :] = jnp.concatenate([lat[0:32], lat[32:64]], axis=1)

    project((-1, 0, 1))
    early = latbuf.at[t, 0:96, :]
    for k, peer in enumerate((xup, xfar, xdn)):
        send(early, early, l_ssem, l_rsem.at[k], peer)
    send(early, early, l_ssem, ld_rsem, partner)
    for k, part in enumerate((left, right)):
        for half, rsem in ((0, up_rsem), (1, dn_rsem)):
            piece = rows_of(chip(2), c, half, part)
            arrived(piece, rsem.at[3 + k])
            send(piece, piece, x_ssem, d_rsem.at[1], partner)
    arrived(xbuf.at[0:32, :], d_rsem.at[1])
    project((2,))
    late = latbuf.at[t, 96:128, :]
    for peer in (xfar, across[2], xup, xdn, across[0], across[1], partner):
        send(late, late, l_ssem, l_rsem.at[3], peer)

    for k in range(3, 11):
        loaded(k)
    signal = dot(xbuf[...], wa[:, 0:256])
    recur = signal[:, 0:128].astype(BF16)
    halo_tx[...] = recur[240:256]
    halo = remote(halo_tx, halo_rx, h_sem.at[0], h_sem.at[1], zup)
    pl.when(z < NZ - 1)(lambda: halo.start())
    gate_s[...] = silu(signal[:, 128:256].astype(BF16).astype(F32))
    rest = dot(xbuf[...], wa[:, 256:512])
    agate_s[...] = silu(rest[:, 0:128].astype(BF16).astype(F32))

    base, far_row = tables[0:TOK, :], tables[pl.ds(TOK + z, 1), :]
    ca, sa, cb, sb = base[:, 0:128], base[:, 128:256], far_row[:, 0:128], far_row[:, 128:256]
    cosine, sine = ca * cb - sa * sb, sa * cb + ca * sb
    lane = lax.broadcasted_iota(jnp.int32, (TOK, 128), 1)
    first = lax.rem(lane, 64) < 32

    def rotated(v):
        swapped = jnp.where(first, -pltpu.roll(v, 96, 1), pltpu.roll(v, 32, 1))
        return v * cosine + swapped * sine

    q_nope = rest[:, 128:256].astype(BF16).astype(F32)
    qr_rk = pbuf[...].astype(F32)
    q_half = jnp.where(lane < 64, qr_rk, 0.0)
    square = jnp.sum(q_nope * q_nope, axis=1, keepdims=True) + jnp.sum(
        q_half * q_half, axis=1, keepdims=True
    )
    scale = lax.rsqrt(square * (1.0 / 192.0) + EPS)
    qgain_rope = jnp.concatenate([qgain[:, 128:192], jnp.ones((1, 64), F32)], axis=1)
    q_nope = q_nope * scale * qgain[:, 0:128]
    turned = rotated(qr_rk * jnp.where(lane < 64, scale * qgain_rope, 1.0))
    zero64 = jnp.zeros((64, TOK), BF16)
    qn_s[...] = jnp.transpose(q_nope).astype(BF16)
    q_rope_t = jnp.transpose(turned)[0:64].astype(BF16)
    qlo_s[...] = jnp.concatenate([q_rope_t, zero64], axis=0)
    qhi_s[...] = jnp.concatenate([zero64, q_rope_t], axis=0)
    key_rope = turned[:, 64:128].astype(BF16)

    for k, o in enumerate((-1, -2, -3)):
        slot = latbuf.at[tp_of(chip(o), c), 0:96, :]
        arrived(slot, l_rsem.at[k])
        send(slot, slot, l_ssem, ld_rsem, partner)
    arrived(latbuf.at[0:4, 0:96, :], ld_rsem)
    arrived(latbuf.at[0:7, 0:32, :], l_rsem.at[3])
    rows = []
    for g in range(4):
        for lanes in (slice(0, 64), slice(64, 128)):
            rows.append(
                jnp.concatenate(
                    [
                        latbuf[k, r : r + 32, lanes]
                        for k in range(8)
                        for r in (32 * ((g - k // 2 + 1) % 4),)
                    ],
                    axis=1,
                )
            )
    latent = jnp.concatenate(rows, axis=0).astype(F32)
    lgain = jnp.concatenate([small[k : k + 1, :] for k in range(4, 8)], axis=1)
    latent = latent * lax.rsqrt(jnp.mean(latent * latent, axis=1, keepdims=True) + EPS) * lgain
    kv = dot(latent.astype(BF16), lup[...])
    k_nope = kv[:, 0:128].astype(BF16)
    v_t = jnp.transpose(kv[:, 128:256]).astype(BF16)
    for h in range(2):
        r, p0 = 64 + 256 * h, 128 * h
        kvbuf[z, r : r + 128, :] = k_nope[p0 : p0 + 128]
        kvbuf[z, r + 128 : r + 256, :] = v_t[:, p0 : p0 + 128]
        kvbuf[z, 576 * h : 576 * h + 64, :] = jnp.concatenate(
            [key_rope[p0 : p0 + 64], key_rope[p0 + 64 : p0 + 128]], axis=1
        )

    def piece_at(slot, k):
        p = k + c * (PIECES - 1 - 2 * k)
        return kvbuf.at[slot, pl.ds(pl.multiple_of(64 * c + ROWS * p, 16), ROWS), :]

    def forward(step, slot, direction, k):
        piece = piece_at(slot, k)
        if direction == 0:
            send(piece, piece, up_ssem.at[step], upkv_rsem.at[step, k], zup)
        else:
            send(piece, piece, dn_ssem.at[step], dnkv_rsem.at[step, k], zdn)

    def carry_on(step, slot, direction):
        carry = cbuf.at[slot]
        ssem, to = (up_ssem, zup) if direction == 0 else (dn_ssem, zdn)
        send(carry, carry, ssem.at[step], c_rsem.at[direction, step], to)

    def shared(slot, core):
        return kvbuf.at[slot, pl.ds(pl.multiple_of(576 * core, 64), 64), :]

    def share(step, slot, direction):
        return remote(
            shared(slot, c), shared(slot, c), s_ssem.at[direction, step],
            s_rsem.at[direction, step], partner,
        )

    sends_up = z < NZ - 1
    for k in range(PIECES):
        pl.when(sends_up)(lambda: forward(0, z, 0, k))
        pl.when(z < (DOWN + 1 if k < HALF else DOWN))(lambda: forward(0, z, 1, PIECES - 1 - k))

    row = lax.broadcasted_iota(jnp.int32, (TOK, 128), 0)
    pl.when(z > 0)(lambda: arrived(halo_rx, h_sem.at[1]))
    behind = jnp.where(z > 0, halo_rx[...].astype(F32), 0.0)
    recur = recur.astype(F32)
    conv_sum = None
    for tap in range(4):
        back = 3 - tap
        if back:
            moved = pltpu.roll(recur, back, 0)
            edge = pltpu.roll(behind, back, 0)
            edge = jnp.concatenate([edge[0:8], moved[8:TOK]], axis=0)
            term = jnp.where(row < back, edge, moved)
        else:
            term = recur
        term = conv[tap : tap + 1, :] * term
        conv_sum = term if conv_sum is None else conv_sum + term
    conv_out = conv_sum.astype(BF16)
    zb = jnp.zeros((64, 64), BF16)

    def diagonal(w):
        return jnp.concatenate(
            [jnp.concatenate([w[0], zb], axis=1), jnp.concatenate([zb, w[1]], axis=1)], axis=0
        )

    recur_rate = jax.nn.sigmoid(dot(conv_out, diagonal(blocks[0:2])))
    input_rate = jax.nn.sigmoid(dot(conv_out, diagonal(blocks[2:4])))
    shift = jnp.concatenate(
        [
            jnp.transpose(jnp.broadcast_to(small[k : k + 1, :], (128, 128)))
            for k in (2, 3)
        ],
        axis=0,
    )
    log_decay = -8.0 * recur_rate * small[0:1, :] + shift
    a = jnp.exp(log_decay)
    b = jnp.sqrt(minus_expm1(2.0 * log_decay)) * input_rate * conv_out.astype(F32)
    for back in (1, 2, 4, 8, 16, 32, 64, 128):
        inside = row >= back
        a_before = jnp.where(inside, pltpu.roll(a, back, 0), 1.0)
        b_before = jnp.where(inside, pltpu.roll(b, back, 0), 0.0)
        b = a * b_before + b
        a = a * a_before
    a_s[...] = a
    b_s[...] = b
    cbuf[z] = jnp.concatenate([a[TOK - 1 : TOK], b[TOK - 1 : TOK], jnp.zeros((6, 128), F32)], axis=0)
    pl.when(sends_up)(lambda: carry_on(0, z, 0))
    pl.when(z < DOWN)(lambda: carry_on(0, z, 1))

    to_exp2 = float(192 ** -0.5 * np.log2(np.e))

    def scores(slot, h):
        r = 64 + 256 * h
        rope = kvbuf[slot, 576 * h : 576 * h + 64, :]
        s = dot(kvbuf[slot, r : r + 128, :], qn_s[...])
        s = s + jnp.concatenate([dot(rope, qlo_s[...]), dot(rope, qhi_s[...])], axis=0)
        return s * to_exp2

    def values(slot, h, weights):
        r = 64 + 256 * h
        return dot(kvbuf[slot, r + 128 : r + 256, :], weights.astype(BF16))

    key = lax.broadcasted_iota(jnp.int32, (128, TOK), 0)
    query = lax.broadcasted_iota(jnp.int32, (128, TOK), 1)
    s = [jnp.where(key + 128 * h <= query, scores(z, h), -jnp.inf) for h in range(2)]
    m = jnp.maximum(jnp.max(s[0], axis=0, keepdims=True), jnp.max(s[1], axis=0, keepdims=True))
    w = [jnp.exp2(v - m) for v in s]
    ml_s[0:1, :] = m
    ml_s[1:2, :] = jnp.sum(w[0] + w[1], axis=0, keepdims=True)
    acc_s[...] = values(z, 0, w[0]) + values(z, 1, w[1])

    def attend(step, slot, direction):
        @pl.when(slot < z)
        def _():
            arrived(shared(slot, 1 - c), s_rsem.at[direction, step])
            s = [scores(slot, h) for h in range(2)]
            old = ml_s[0:1, :]
            m = jnp.maximum(old, jnp.max(jnp.maximum(s[0], s[1]), axis=0, keepdims=True))
            w = [jnp.exp2(v - m) for v in s]
            rescale = jnp.exp2(old - m)
            ml_s[0:1, :] = m
            ml_s[1:2, :] = ml_s[1:2, :] * rescale + jnp.sum(w[0] + w[1], axis=0, keepdims=True)
            acc_s[...] = acc_s[...] * rescale + (values(slot, 0, w[0]) + values(slot, 1, w[1]))

    def step(s, before, last=False):
        up, dn = zat(-s), zat(s)
        has_up, has_dn = s <= z, dn < DOWN
        for k in range(PIECES):
            q = PIECES - 1 - k

            if k < HALF or not last:

                @pl.when(has_up)
                def _():
                    arrived(piece_at(up, k), upkv_rsem.at[s - 1, k])
                    if not last:
                        goes = sends_up & (s < DOWN) if k >= HALF else sends_up
                        pl.when(goes)(lambda: forward(s, up, 0, k))
                    if k == 0:
                        share(s - 1, up, 0).start()

                @pl.when((dn <= DOWN) if k < HALF else has_dn)
                def _():
                    arrived(piece_at(dn, q), dnkv_rsem.at[s - 1, q])
                    if not last:
                        if k < HALF:
                            forward(s, dn, 1, q)
                        else:
                            pl.when(s < DOWN)(lambda: forward(s, dn, 1, q))
                    if q == 0:
                        pl.when(dn < z)(lambda: share(s - 1, dn, 1).start())

            if before and k == 1:
                attend(s - 2, zat(1 - s), 0)
            if before and k == 3:
                attend(s - 2, zat(s - 1), 1)

        @pl.when(has_up)
        def _():
            arrived(cbuf.at[up], c_rsem.at[0, s - 1])
            if not last:
                pl.when(sends_up)(lambda: carry_on(s, up, 0))

        if not last:

            @pl.when(has_dn)
            def _():
                arrived(cbuf.at[dn], c_rsem.at[1, s - 1])
                pl.when(s < DOWN)(lambda: carry_on(s, dn, 1))

    offsets = (2, 1, -1, 0)

    def finish():
        def onward(j, state):
            return cbuf[j, 0:1, :] * state + cbuf[j, 1:2, :]

        incoming = lax.fori_loop(0, z, onward, small[1:2, :])
        xrow[:, 0:128] = ((b_s[...] + a_s[...] * incoming) * gate_s[...]).astype(BF16)
        attended = jnp.transpose(acc_s[...] / ml_s[1:2, :])
        xrow[:, 128:256] = (attended * agate_s[...]).astype(BF16)
        for side, cc in enumerate((1 - c, c)):
            for k, o in enumerate(offsets):
                at = pl.multiple_of(32 * tp_of(chip(o), cc), 32)
                xcat[side, 32 * k : 32 * k + 32, :] = xrow[pl.ds(at, 32), :]
        d2d_tx[...] = dot(xcat[0], wo[...]).astype(BF16)
        for k in range(4):
            part = slice(32 * k, 32 * k + 32)
            send(d2d_tx.at[part, :], d2d_rx.at[part, :], o_ssem, o_rsem.at[k], partner)
        psum[...] = dot(xcat[1], wo[...])

    def ship(k, value, to):
        width = value.shape[1]
        rtx[k, :, 0:width] = value.astype(BF16)
        send(rtx.at[k, :, 0:width], rrx.at[k, :, 0:width], r_ssem, r_rsem.at[k], to)

    def landed(k, width=512):
        arrived(rrx.at[k, :, 0:width], r_rsem.at[k])
        return rrx[k, :, 0:width].astype(F32)

    def add_partner(k):
        part = slice(32 * k, 32 * k + 32)
        arrived(d2d_rx.at[part, :], o_rsem.at[k])
        both = psum[part, :] + d2d_rx[part, :].astype(F32)
        psum[part, :] = both
        return both

    def reduce_first():
        two = add_partner(0)
        ship(0, two[:, 0:512], xup)
        ship(5, two[:, 1024:1536], xdn)
        ship(1, two[:, 512:1024], xup)
        ship(6, two[:, 1536:2048], xdn)
        ship(2, add_partner(1)[:, 1024:2048], xup)
        ship(7, add_partner(2)[:, 0:1024], xdn)

    def reduce_second():
        for k in range(2):
            at = 512 * k
            ship(3 + k, psum[32:64, at : at + 512] + landed(k), xup)
            ship(8 + k, psum[64:96, 1024 + at : 1536 + at] + landed(5 + k), xdn)

    def reduce_last():
        add_partner(3)
        direct = (landed(7, 1024), landed(2, 1024))
        for k in range(2):
            for side in range(2):
                at = 1024 * side + 512 * k
                total = psum[96:128, at : at + 512] + direct[side][:, 512 * k : 512 * k + 512]
                out_ref[:, at : at + 512] = (total + landed((3, 8)[side] + k)).astype(BF16)

    def between(when, stage):
        pl.when((z < 2) & when)(stage)

    step(1, False)

    def middle(s, _):
        step(s, True)
        between(s == 2, finish)
        between(s == 3, reduce_first)
        between(s == 4, reduce_second)
        between(s == 5, reduce_last)
        return 0

    lax.fori_loop(2, UP, middle, 0)
    step(UP, True, last=True)
    attend(UP - 1, zat(-UP), 0)

    @pl.when(z >= 2)
    def _():
        finish()
        reduce_first()
        reduce_second()
        reduce_last()


    @pl.when(sends_up)
    def _():
        sent(halo_tx, h_sem.at[0])

    def drain(s, _):
        dn = zat(s)
        first, full = pl.ds(0, HALF * ROWS), pl.ds(0, PIECES * ROWS + 16)

        @pl.when(sends_up & (s <= z))
        def _():
            pl.when(s < DOWN)(lambda: sent(kvbuf.at[0, full, :], up_ssem.at[s]))
            pl.when(s == DOWN)(
                lambda: sent(kvbuf.at[0, pl.ds(0, HALF * ROWS + 16), :], up_ssem.at[s])
            )

        whole = (dn < DOWN) & (s < DOWN)
        pl.when(whole)(lambda: sent(kvbuf.at[0, full, :], dn_ssem.at[s]))
        pl.when((dn <= DOWN) & jnp.logical_not(whole))(
            lambda: sent(kvbuf.at[0, first, :], dn_ssem.at[s])
        )
        pl.when(zat(-1 - s) < z)(lambda: sent(shared(0, c), s_ssem.at[0, s]))
        pl.when((zat(1 + s) < z) & (s < DOWN))(lambda: sent(shared(0, c), s_ssem.at[1, s]))
        return 0

    lax.fori_loop(0, UP, drain, 0)
    sent(xbuf.at[0:224, :], x_ssem)
    sent(latbuf.at[0:7, :, :], l_ssem)
    sent(d2d_tx, o_ssem)
    sent(rtx.at[0:6, :, :], r_ssem)


def body(
    tokens, norm_gain, recurrent_input, recurrent_gate, attention_gate, query_proj, latent_down,
    rope_key_down, conv_kernel, recurrence_gate_blocks, input_gate_blocks, decay_rate,
    decay_shift, initial_state, latent_gain, latent_up, query_gain, recurrent_output,
    attention_output,
):
    base, far = (jnp.asarray(v) for v in rotary_tables())

    def row(v):
        return v.reshape(1, -1)

    operands = (
        tokens, row(norm_gain), recurrent_input, recurrent_gate, attention_gate, query_proj.T,
        latent_down.T, rope_key_down.T, conv_kernel, recurrence_gate_blocks, input_gate_blocks,
        row(decay_rate), decay_shift.reshape(2, 128), row(initial_state),
        latent_gain.reshape(4, 128), latent_up,
        row(query_gain), recurrent_output, attention_output, base, far,
    )
    dma, vmem = pltpu.SemaphoreType.DMA, pltpu.VMEM
    scratch = [
        vmem((32, D), BF16), vmem((1, D), F32), vmem((D, 512), BF16), vmem((D, 256), BF16),
        vmem((384, D), BF16), vmem((4, 128), F32), vmem((4, 64, 64), BF16), vmem((8, 128), F32),
        vmem((512, 256), BF16), vmem((1, 192), F32), vmem((256, D), BF16),
        vmem((TOK + NZ, 256), F32),
        vmem((TOK, D), BF16), vmem((TOK, 128), BF16), vmem((8, 128, 128), BF16),
        vmem((16, 128), BF16), vmem((16, 128), BF16), vmem((NZ, 640, 128), BF16),
        vmem((NZ, 8, 128), F32), vmem((128, TOK), BF16), vmem((128, TOK), BF16),
        vmem((128, TOK), BF16), vmem((128, TOK), F32), vmem((8, TOK), F32),
        vmem((TOK, 128), F32), vmem((TOK, 128), F32), vmem((TOK, 128), F32),
        vmem((TOK, 128), F32), vmem((TOK, 256), BF16), vmem((2, 128, 256), BF16),
        vmem((128, D), BF16), vmem((128, D), BF16), vmem((128, D), F32),
        vmem((10, 32, 1024), BF16), vmem((10, 32, 1024), BF16),
        dma((11,)), dma(()), dma((5,)), dma((5,)), dma((2,)), dma(()), dma((4,)), dma(()),
        dma((2,)), dma((8,)), dma((8,)), dma((8, PIECES)), dma((8, PIECES)), dma((2, 8)),
        dma((2, 8)), dma((2, 8)), dma(()), dma((4,)), dma(()), dma((10,)),
    ]
    return pl.pallas_call(
        kernel,
        out_shape=pltpu.VMEM((32, D), BF16),
        in_specs=[pl.BlockSpec(memory_space=pl.ANY)] * len(operands),
        scratch_shapes=scratch,
        compiler_params=pltpu.CompilerParams(
            collective_id=0, has_side_effects=True, vmem_limit_bytes=56 * 2**20
        ),
    )(*operands)


def solution(mesh):
    return jax.shard_map(
        body,
        mesh=mesh,
        in_specs=(
            P(("fs", "sp", "tp"), None), P(), P(None, "tp"), P(None, "tp"), P(None, "tp"),
            P(None, "tp"), P(None, "tp"), P(), P(None, "tp"), P("tp", None, None),
            P("tp", None, None), P("tp"), P(("fs", "sp")), P(("fs", "tp")), P(), P(None, "tp"),
            P(), P("tp", None), P("tp", None),
        ),
        out_specs=P(("fs", "sp", "tp"), None),
        check_vma=False,
    )
```

time: 62.3 us -> 58.7 us (0.942)
  the two profiles are of different devices: /device:TPU:408 before, /device:TPU:393 now
where the time goes in v3:
time: 58.7 us; the launch traced here: 58.6 us
  Pallas kernels  58 us (99%)
  local copies, waits for them, and re-layouts  0.66 us (1%)
    pallas_call x1, Pallas kernels, body(): pl.pallas_call(kernel, out_shape=pltpu.VMEM((32, D), BF16), in_specs=[pl....  58 us

profile of v3, /device:TPU:393, one launch (start us, length us, event | category | flops | bytes accessed | tf_op | source)
XLA Modules:
  0.0 58.6 jit_solution(3578088071002260624)
XLA Ops:
  0.0 58.0 %shard_map.199 = bf16[32,2048]{1,0:T(8,128)(2,1)S(1)} custom-call(bf16[32,2048]{1,0:T(8,128)(2,1)} %tok_h.1, f32[1,2048]{1,0:T(1,128)} %bitcast.12, bf16[2048,128]{1,0:T(8,128)(2,1)} %rin_h.1, bf16[2048,128]{1,0:T(8,128)(2,1)} %rgate_h.1, bf16[2048,128]{1,0:T(8,128)(2,1)} %agate_h.1, bf16[192,2048]{1,0:T(8,128)(2,1)} %bitcast.9, bf16[64,2048]{1,0:T(8,128)(2,1)} %bitcast.10, ...), custom_call_target="tpu_custom_call" | custom-call | tf_op jit(solution)/shard_map/pallas_call | solution.py:568
  58.0 0.7 %copy.23 = bf16[32,2048]{1,0:T(8,128)(2,1)} copy(bf16[32,2048]{1,0:T(8,128)(2,1)S(1)} %shard_map.199) | data formatting | bytes 262144

commit v4 on v3

--- a/solution.py
+++ b/solution.py
@@ -13,7 +13,8 @@
 THETA = 10000.0
 F32, BF16 = jnp.float32, jnp.bfloat16
 NZ, NX, TOK, D = 16, 4, 256, 2048
-PIECES, HALF, ROWS = 6, 3, 96
+PARTS = ((0, 96), (96, 80), (176, 80), (256, 96), (352, 80), (432, 80))
+PIECES, HALF = 6, 3
 UP, DOWN = 8, 7
 NT = (((1,), (1,)), ((), ()))
 
@@ -50,9 +51,9 @@
     out_ref,
     tok, ngain, wa, wb, wt, conv, blocks, small, lup, qgain, wo, tables,
     xbuf, pbuf, latbuf, halo_tx, halo_rx, kvbuf, cbuf, qn_s, qlo_s, qhi_s, acc_s, ml_s,
-    a_s, b_s, gate_s, agate_s, xrow, xcat, d2d_tx, d2d_rx, psum, rtx, rrx,
+    a_s, b_s, gate_s, agate_s, xrow, xcat, d2d_tx, d2d_rx, psum, rtx, rrx, ropebuf,
     in_sem, x_ssem, up_rsem, dn_rsem, d_rsem, l_ssem, l_rsem, ld_rsem, h_sem,
-    up_ssem, dn_ssem, upkv_rsem, dnkv_rsem, s_ssem, s_rsem, c_rsem, o_ssem, o_rsem, r_ssem, r_rsem,
+    up_ssem, dn_ssem, upkv_rsem, dnkv_rsem, s_ssem, s_rsem, rr_sem, c_ssem, c_rsem, o_ssem, o_rsem, r_ssem, r_rsem,
 ):
     z = lax.axis_index("sp")
     t = lax.axis_index("tp")
@@ -194,6 +195,51 @@
     rest = dot(xbuf[...], wa[:, 256:512])
     agate_s[...] = silu(rest[:, 0:128].astype(BF16).astype(F32))
 
+    sends_up = z < NZ - 1
+
+    def piece_at(slot, k):
+        return kvbuf.at[slot, pl.ds(*PARTS[k]), :]
+
+    def onward(direction, what, step, rsem):
+        if direction == 0:
+            send(what, what, up_ssem.at[step], rsem, zup)
+        else:
+            send(what, what, dn_ssem.at[step], rsem, zdn)
+
+    def forward(step, slot, direction, k):
+        rsem = upkv_rsem if direction == 0 else dnkv_rsem
+        onward(direction, piece_at(slot, k), step, rsem.at[step, k])
+
+    def carry_on(step, slot, direction):
+        carry = cbuf.at[slot]
+        rsem, to = c_rsem.at[direction, step], (zup, zdn)[direction]
+        send(carry, carry, c_ssem.at[direction, step], rsem, to)
+
+    own_sixteenth = pl.ds(pl.multiple_of(16 * t, 16), 16)
+
+    def rope_on(step, slot, direction):
+        onward(direction, ropebuf.at[slot, own_sixteenth, :], step, rr_sem.at[direction, step])
+
+    def share(step, slot, direction):
+        mine = ropebuf.at[slot, own_sixteenth, :]
+        for peer in (xfar, across[2], xup, xdn, across[0], across[1], partner):
+            send(mine, mine, s_ssem.at[direction, step], s_rsem.at[direction, step], peer)
+
+    def rope_step(s):
+        up, dn = zat(-s), zat(s)
+
+        @pl.when((s <= z) & (s <= UP))
+        def _():
+            arrived(ropebuf.at[up, own_sixteenth, :], rr_sem.at[0, s - 1])
+            pl.when(sends_up & (s < UP))(lambda: rope_on(s, up, 0))
+            share(s - 1, up, 0)
+
+        @pl.when((dn < DOWN) & (s <= DOWN))
+        def _():
+            arrived(ropebuf.at[dn, own_sixteenth, :], rr_sem.at[1, s - 1])
+            pl.when(s < DOWN)(lambda: rope_on(s, dn, 1))
+            pl.when(dn < z)(lambda: share(s - 1, dn, 1))
+
     base, far_row = tables[0:TOK, :], tables[pl.ds(TOK + z, 1), :]
     ca, sa, cb, sb = base[:, 0:128], base[:, 128:256], far_row[:, 0:128], far_row[:, 128:256]
     cosine, sine = ca * cb - sa * sb, sa * cb + ca * sb
@@ -220,6 +266,13 @@
     qlo_s[...] = jnp.concatenate([q_rope_t, zero64], axis=0)
     qhi_s[...] = jnp.concatenate([zero64, q_rope_t], axis=0)
     key_rope = turned[:, 64:128].astype(BF16)
+    for h in range(2):
+        p0 = 128 * h
+        ropebuf[z, 64 * h : 64 * h + 64, :] = jnp.concatenate(
+            [key_rope[p0 : p0 + 64], key_rope[p0 + 64 : p0 + 128]], axis=1
+        )
+    pl.when(sends_up)(lambda: rope_on(0, z, 0))
+    pl.when(z < DOWN)(lambda: rope_on(0, z, 1))
 
     for k, o in enumerate((-1, -2, -3)):
         slot = latbuf.at[tp_of(chip(o), c), 0:96, :]
@@ -247,42 +300,13 @@
     k_nope = kv[:, 0:128].astype(BF16)
     v_t = jnp.transpose(kv[:, 128:256]).astype(BF16)
     for h in range(2):
-        r, p0 = 64 + 256 * h, 128 * h
+        r, p0 = 256 * h, 128 * h
         kvbuf[z, r : r + 128, :] = k_nope[p0 : p0 + 128]
         kvbuf[z, r + 128 : r + 256, :] = v_t[:, p0 : p0 + 128]
-        kvbuf[z, 576 * h : 576 * h + 64, :] = jnp.concatenate(
-            [key_rope[p0 : p0 + 64], key_rope[p0 + 64 : p0 + 128]], axis=1
-        )
-
-    def piece_at(slot, k):
-        p = k + c * (PIECES - 1 - 2 * k)
-        return kvbuf.at[slot, pl.ds(pl.multiple_of(64 * c + ROWS * p, 16), ROWS), :]
-
-    def forward(step, slot, direction, k):
-        piece = piece_at(slot, k)
-        if direction == 0:
-            send(piece, piece, up_ssem.at[step], upkv_rsem.at[step, k], zup)
-        else:
-            send(piece, piece, dn_ssem.at[step], dnkv_rsem.at[step, k], zdn)
-
-    def carry_on(step, slot, direction):
-        carry = cbuf.at[slot]
-        ssem, to = (up_ssem, zup) if direction == 0 else (dn_ssem, zdn)
-        send(carry, carry, ssem.at[step], c_rsem.at[direction, step], to)
-
-    def shared(slot, core):
-        return kvbuf.at[slot, pl.ds(pl.multiple_of(576 * core, 64), 64), :]
-
-    def share(step, slot, direction):
-        return remote(
-            shared(slot, c), shared(slot, c), s_ssem.at[direction, step],
-            s_rsem.at[direction, step], partner,
-        )
-
-    sends_up = z < NZ - 1
-    for k in range(PIECES):
+
+    for k in range(HALF):
         pl.when(sends_up)(lambda: forward(0, z, 0, k))
-        pl.when(z < (DOWN + 1 if k < HALF else DOWN))(lambda: forward(0, z, 1, PIECES - 1 - k))
+        pl.when(z <= DOWN)(lambda: forward(0, z, 1, PIECES - 1 - k))
 
     row = lax.broadcasted_iota(jnp.int32, (TOK, 128), 0)
     pl.when(z > 0)(lambda: arrived(halo_rx, h_sem.at[1]))
@@ -328,21 +352,25 @@
         a = a * a_before
     a_s[...] = a
     b_s[...] = b
-    cbuf[z] = jnp.concatenate([a[TOK - 1 : TOK], b[TOK - 1 : TOK], jnp.zeros((6, 128), F32)], axis=0)
+    rope_step(1)
+    for k in range(HALF):
+        pl.when(sends_up)(lambda: forward(0, z, 0, HALF + k))
+        pl.when(z < DOWN)(lambda: forward(0, z, 1, HALF - 1 - k))
+    cbuf[z] = jnp.concatenate([a[TOK - 1 : TOK], b[TOK - 1 : TOK]], axis=0)
     pl.when(sends_up)(lambda: carry_on(0, z, 0))
     pl.when(z < DOWN)(lambda: carry_on(0, z, 1))
 
     to_exp2 = float(192 ** -0.5 * np.log2(np.e))
 
     def scores(slot, h):
-        r = 64 + 256 * h
-        rope = kvbuf[slot, 576 * h : 576 * h + 64, :]
+        r = 256 * h
+        rope = ropebuf[slot, 64 * h : 64 * h + 64, :]
         s = dot(kvbuf[slot, r : r + 128, :], qn_s[...])
         s = s + jnp.concatenate([dot(rope, qlo_s[...]), dot(rope, qhi_s[...])], axis=0)
         return s * to_exp2
 
     def values(slot, h, weights):
-        r = 64 + 256 * h
+        r = 256 * h
         return dot(kvbuf[slot, r + 128 : r + 256, :], weights.astype(BF16))
 
     key = lax.broadcasted_iota(jnp.int32, (128, TOK), 0)
@@ -357,7 +385,7 @@
     def attend(step, slot, direction):
         @pl.when(slot < z)
         def _():
-            arrived(shared(slot, 1 - c), s_rsem.at[direction, step])
+            arrived(ropebuf.at[slot, 0:112, :], s_rsem.at[direction, step])
             s = [scores(slot, h) for h in range(2)]
             old = ml_s[0:1, :]
             m = jnp.maximum(old, jnp.max(jnp.maximum(s[0], s[1]), axis=0, keepdims=True))
@@ -381,8 +409,6 @@
                     if not last:
                         goes = sends_up & (s < DOWN) if k >= HALF else sends_up
                         pl.when(goes)(lambda: forward(s, up, 0, k))
-                    if k == 0:
-                        share(s - 1, up, 0).start()
 
                 @pl.when((dn <= DOWN) if k < HALF else has_dn)
                 def _():
@@ -392,13 +418,13 @@
                             forward(s, dn, 1, q)
                         else:
                             pl.when(s < DOWN)(lambda: forward(s, dn, 1, q))
-                    if q == 0:
-                        pl.when(dn < z)(lambda: share(s - 1, dn, 1).start())
 
             if before and k == 1:
                 attend(s - 2, zat(1 - s), 0)
             if before and k == 3:
                 attend(s - 2, zat(s - 1), 1)
+            if k == 2 and not last:
+                rope_step(s + 1)
 
         @pl.when(has_up)
         def _():
@@ -416,10 +442,10 @@
     offsets = (2, 1, -1, 0)
 
     def finish():
-        def onward(j, state):
+        def folded(j, state):
             return cbuf[j, 0:1, :] * state + cbuf[j, 1:2, :]
 
-        incoming = lax.fori_loop(0, z, onward, small[1:2, :])
+        incoming = lax.fori_loop(0, z, folded, small[1:2, :])
         xrow[:, 0:128] = ((b_s[...] + a_s[...] * incoming) * gate_s[...]).astype(BF16)
         attended = jnp.transpose(acc_s[...] / ml_s[1:2, :])
         xrow[:, 128:256] = (attended * agate_s[...]).astype(BF16)
@@ -474,15 +500,15 @@
                 out_ref[:, at : at + 512] = (total + landed((3, 8)[side] + k)).astype(BF16)
 
     def between(when, stage):
-        pl.when((z < 2) & when)(stage)
-
+        pl.when((z == 0) & when)(stage)
+
+    pl.when(z == 0)(finish)
     step(1, False)
+    pl.when(z == 0)(reduce_first)
 
     def middle(s, _):
         step(s, True)
-        between(s == 2, finish)
-        between(s == 3, reduce_first)
-        between(s == 4, reduce_second)
+        between(s == 3, reduce_second)
         between(s == 5, reduce_last)
         return 0
 
@@ -490,7 +516,7 @@
     step(UP, True, last=True)
     attend(UP - 1, zat(-UP), 0)
 
-    @pl.when(z >= 2)
+    @pl.when(z > 0)
     def _():
         finish()
         reduce_first()
@@ -504,22 +530,28 @@
 
     def drain(s, _):
         dn = zat(s)
-        first, full = pl.ds(0, HALF * ROWS), pl.ds(0, PIECES * ROWS + 16)
+        half, block = pl.ds(0, 256), pl.ds(0, 528)
 
         @pl.when(sends_up & (s <= z))
         def _():
-            pl.when(s < DOWN)(lambda: sent(kvbuf.at[0, full, :], up_ssem.at[s]))
-            pl.when(s == DOWN)(
-                lambda: sent(kvbuf.at[0, pl.ds(0, HALF * ROWS + 16), :], up_ssem.at[s])
-            )
+            pl.when(s < DOWN)(lambda: sent(kvbuf.at[0, block, :], up_ssem.at[s]))
+            pl.when(s == DOWN)(lambda: sent(kvbuf.at[0, pl.ds(0, 272), :], up_ssem.at[s]))
+            sent(cbuf.at[0], c_ssem.at[0, s])
 
         whole = (dn < DOWN) & (s < DOWN)
-        pl.when(whole)(lambda: sent(kvbuf.at[0, full, :], dn_ssem.at[s]))
+
+        @pl.when(whole)
+        def _():
+            sent(kvbuf.at[0, block, :], dn_ssem.at[s])
+            sent(cbuf.at[0], c_ssem.at[1, s])
+
         pl.when((dn <= DOWN) & jnp.logical_not(whole))(
-            lambda: sent(kvbuf.at[0, first, :], dn_ssem.at[s])
+            lambda: sent(kvbuf.at[0, half, :], dn_ssem.at[s])
         )
-        pl.when(zat(-1 - s) < z)(lambda: sent(shared(0, c), s_ssem.at[0, s]))
-        pl.when((zat(1 + s) < z) & (s < DOWN))(lambda: sent(shared(0, c), s_ssem.at[1, s]))
+        pl.when(zat(-1 - s) < z)(lambda: sent(ropebuf.at[0, 0:112, :], s_ssem.at[0, s]))
+        pl.when((zat(1 + s) < z) & (s < DOWN))(
+            lambda: sent(ropebuf.at[0, 0:112, :], s_ssem.at[1, s])
+        )
         return 0
 
     lax.fori_loop(0, UP, drain, 0)
@@ -554,16 +586,16 @@
         vmem((512, 256), BF16), vmem((1, 192), F32), vmem((256, D), BF16),
         vmem((TOK + NZ, 256), F32),
         vmem((TOK, D), BF16), vmem((TOK, 128), BF16), vmem((8, 128, 128), BF16),
-        vmem((16, 128), BF16), vmem((16, 128), BF16), vmem((NZ, 640, 128), BF16),
-        vmem((NZ, 8, 128), F32), vmem((128, TOK), BF16), vmem((128, TOK), BF16),
+        vmem((16, 128), BF16), vmem((16, 128), BF16), vmem((NZ, 528, 128), BF16),
+        vmem((NZ, 2, 128), F32), vmem((128, TOK), BF16), vmem((128, TOK), BF16),
         vmem((128, TOK), BF16), vmem((128, TOK), F32), vmem((8, TOK), F32),
         vmem((TOK, 128), F32), vmem((TOK, 128), F32), vmem((TOK, 128), F32),
         vmem((TOK, 128), F32), vmem((TOK, 256), BF16), vmem((2, 128, 256), BF16),
         vmem((128, D), BF16), vmem((128, D), BF16), vmem((128, D), F32),
-        vmem((10, 32, 1024), BF16), vmem((10, 32, 1024), BF16),
+        vmem((10, 32, 1024), BF16), vmem((10, 32, 1024), BF16), vmem((NZ, 128, 128), BF16),
         dma((11,)), dma(()), dma((5,)), dma((5,)), dma((2,)), dma(()), dma((4,)), dma(()),
         dma((2,)), dma((8,)), dma((8,)), dma((8, PIECES)), dma((8, PIECES)), dma((2, 8)),
-        dma((2, 8)), dma((2, 8)), dma(()), dma((4,)), dma(()), dma((10,)),
+        dma((2, 8)), dma((2, 8)), dma((2, 8)), dma((2, 8)), dma(()), dma((4,)), dma(()), dma((10,)),
     ]
     return pl.pallas_call(
         kernel,

time: 58.7 us -> 58 us (0.988)
  Pallas kernels: 58 us -> 57.3 us
    pallas_call x1, Pallas kernels: 58 us -> 57.3 us  [body(): pl.pallas_call(kernel, out_shape=pltpu.VMEM((32, D), BF16), in_specs=[pl....]
where the time goes in v4:
time: 58 us; the launch traced here: 57.9 us
  Pallas kernels  57.3 us (99%)
  local copies, waits for them, and re-layouts  0.66 us (1%)
    pallas_call x1, Pallas kernels, body(): pl.pallas_call(kernel, out_shape=pltpu.VMEM((32, D), BF16), in_specs=[pl....  57.3 us

profile of v4, /device:TPU:393, one launch (start us, length us, event | category | flops | bytes accessed | tf_op | source)
XLA Modules:
  0.0 57.9 jit_solution(7848978357328093856)
XLA Ops:
  0.0 57.3 %shard_map.199 = bf16[32,2048]{1,0:T(8,128)(2,1)S(1)} custom-call(bf16[32,2048]{1,0:T(8,128)(2,1)} %tok_h.1, f32[1,2048]{1,0:T(1,128)} %bitcast.12, bf16[2048,128]{1,0:T(8,128)(2,1)} %rin_h.1, bf16[2048,128]{1,0:T(8,128)(2,1)} %rgate_h.1, bf16[2048,128]{1,0:T(8,128)(2,1)} %agate_h.1, bf16[192,2048]{1,0:T(8,128)(2,1)} %bitcast.9, bf16[64,2048]{1,0:T(8,128)(2,1)} %bitcast.10, ...), custom_call_target="tpu_custom_call" | custom-call | tf_op jit(solution)/shard_map/pallas_call | solution.py:600
  57.3 0.7 %copy.23 = bf16[32,2048]{1,0:T(8,128)(2,1)} copy(bf16[32,2048]{1,0:T(8,128)(2,1)S(1)} %shard_map.199) | data formatting | bytes 262144
